TPU v7x, 32 devices: a whole 2x2x4 slice. The times are simulated.
32 devices in a mesh: rep: 2 (over x), fs: 8 (over z, y), tp: 2 (over core).
Axes of the slice: x: 2, y: 2, z: 4, core: 2. Of those that a mesh axis runs over, the one named last changes fastest.
Arguments:
- tokens: bfloat16 [4096, 2048], P(('rep', 'fs', 'tp')), may hold values from -6 to 6
- mix_gain: float32 [2048], replicated, may hold values from 0.1 to 1.9
- conv_in_weight: bfloat16 [2048, 1024], P('fs', 'tp'), may hold values from -0.125 to 0.125
- gate_outer_weight: bfloat16 [2048, 1024], P('fs', 'tp'), may hold values from -0.125 to 0.125
- gate_inner_weight: bfloat16 [2048, 1024], P('fs', 'tp'), may hold values from -0.125 to 0.125
- conv_taps: float32 [3, 1024], P(None, 'tp'), may hold values from -3.5 to 3.5
- out_weight: bfloat16 [1024, 2048], P('tp', 'fs'), may hold values from -0.1875 to 0.1875
- ff_gain: float32 [2048], replicated, may hold values from 0.1 to 1.9
- up_weight: bfloat16 [2048, 8192], P('fs', 'tp'), may hold values from -0.125 to 0.125
- down_weight: bfloat16 [8192, 2048], P('tp', 'fs'), may hold values from -0.0625 to 0.0625
Outputs:
- layer_out: bfloat16 [4096, 2048], P(('rep', 'fs', 'tp'))
All inputs are finite; a program needn't handle non-finite values.
Results may differ from a plain program's by a relative error of at most 0.023.
Values may be sent and summed in bfloat16 or wider, within the bound.
A program may use at most 128 MiB of HBM per device.

v0:
```python
import functools

import jax
import jax.numpy as jnp
from jax import lax
from jax.experimental import pallas as pl
from jax.experimental.pallas import tpu as pltpu
from jax.sharding import Mesh, PartitionSpec as P

eps = 1e-06


def rms_scale(values, gain):
    widened = values.astype(jnp.float32)
    inverse = lax.rsqrt(jnp.mean(widened * widened, axis=-1, keepdims=True) + eps)
    return (widened * inverse * gain).astype(jnp.bfloat16)


GROUP = ("rep", "near", "tp")


def gather_rows(block, near):
    rows, width = block.shape[0], block.shape[1] // near
    if near > 1:
        block = lax.all_to_all(
            block.reshape(rows, near, width).transpose(1, 0, 2), "near", 0, 0, tiled=True
        ).reshape(near * rows, width)
    return lax.all_gather(block, "far", axis=0, tiled=True)


def own_part(block, axis, rep):
    size = block.shape[axis] // rep
    return lax.dynamic_slice_in_dim(block, lax.axis_index("rep") * size, size, axis)


def on_device(rep, near, tp, tokens, mix_gain, conv_in, outer, inner, taps, out_w, ff_gain, up_w, down_w):
    seq_rows = tokens.shape[0] * tp
    depth = up_w.shape[0]
    parts = [own_part(w, 1, rep) for w in (conv_in, outer, inner)]
    width = parts[0].shape[1] // near
    trio = jnp.concatenate([p.reshape(depth, near, width) for p in parts], 2).reshape(depth, -1)
    trio = gather_rows(trio, near)
    out_part = own_part(out_w, 0, rep)
    out_part = out_part.reshape(near, width, -1).transpose(1, 0, 2).reshape(width, -1)
    out_full = gather_rows(out_part, near).reshape(-1, width, out_w.shape[1])
    up_full = gather_rows(own_part(up_w, 1, rep), near)
    down_part = own_part(down_w, 0, rep)
    hid = down_part.shape[0] // near
    down_part = down_part.reshape(near, hid, -1).transpose(1, 0, 2).reshape(hid, -1)
    down_full = gather_rows(down_part, near).reshape(-1, hid, down_w.shape[1])

    taps = own_part(taps, 1, rep)
    taps = lax.dynamic_slice_in_dim(taps, lax.axis_index("near") * width, width, 1)

    normed = lax.all_gather(rms_scale(tokens, mix_gain), GROUP, axis=0, tiled=True)
    proj = jnp.dot(normed, trio, preferred_element_type=jnp.float32).astype(jnp.bfloat16)
    proj = proj.astype(jnp.float32).reshape(-1, seq_rows, 3 * width)
    gated = proj[..., 2 * width :] * proj[..., :width]
    padded = jnp.pad(gated, ((0, 0), (2, 0), (0, 0)))
    convolved = sum(taps[k] * padded[:, k : seq_rows + k] for k in range(3))
    mixed = (proj[..., width : 2 * width] * convolved).astype(jnp.bfloat16)
    mixed = mixed.reshape(-1, width)

    def project(lefts, rights):
        whole = rights.transpose(1, 0, 2).reshape(lefts.shape[1], -1)
        partial = jnp.dot(lefts, whole, preferred_element_type=jnp.float32)
        return lax.psum_scatter(
            partial.astype(jnp.bfloat16), GROUP, scatter_dimension=0, tiled=True
        ).astype(jnp.float32)

    resid = (tokens.astype(jnp.float32) + project(mixed, out_full)).astype(jnp.bfloat16)
    normed_ff = lax.all_gather(rms_scale(resid, ff_gain), GROUP, axis=0, tiled=True)
    preact = jnp.dot(normed_ff, up_full, preferred_element_type=jnp.float32)
    hidden = jnp.square(jax.nn.relu(preact)).astype(jnp.bfloat16)
    return (resid.astype(jnp.float32) + project(hidden, down_full)).astype(jnp.bfloat16)


def visit_order(far):
    return [sorted(range(far), key=lambda s: (abs(s - z), s)) for z in range(far)]


def layer_kernel(
    far,
    tok_ref, mix_gain_ref, conv_ref, outer_ref, inner_ref, taps_ref, outw_ref, ff_gain_ref, upw_ref, dnw_ref,
    o_ref,
    trio, outb, upb, dnb, stage, toks, toks_ff, part, sib, rsend, rrecv, part_ff, sib_ff, rsend_ff, rrecv_ff,
    hidden, resid,
    local_sem, stage_sem, near_send, right_send, left_send, w_recv,
    ag_send, ag_recv, sib_send, sib_recv, rs_send, rs_recv,
):
    r, z, y, t = (lax.axis_index(name) for name in ("rep", "far", "near", "tp"))
    m = r * 2 + y
    rows = tok_ref.shape[0]
    seq = 2 * rows
    width = trio.shape[1] // 3
    depth, hid = upw_ref.shape[0], upb.shape[1]
    cols = dnw_ref.shape[1]
    bf16, f32 = jnp.bfloat16, jnp.float32

    def al(v, n):
        return pl.multiple_of(v, n)

    def push(a, b, s, q, where):
        return pltpu.make_async_remote_copy(
            src_ref=a, dst_ref=b, send_sem=s, recv_sem=q, device_id=where, device_id_type=pl.DeviceIdType.MESH
        )

    def chip(c):
        return (lax.div(c, 2), z, lax.rem(c, 2), t)

    sibling = (r, z, y, 1 - t)
    beside = (r, z, 1 - y, t)

    def place(k, zs, ys):
        p = zs * 2 + ys
        if k == 0:
            return trio.at[pl.ds(al(p * depth, depth), depth), :]
        if k == 1:
            return outb.at[:, pl.ds(al(p * cols, cols), cols)]
        if k == 2:
            return upb.at[pl.ds(al(p * depth, depth), depth), :]
        return dnb.at[:, pl.ds(al(p * cols, cols), cols)]

    def share(k, ys):
        q = r * 2 + ys
        if k == 1:
            return outw_ref.at[pl.ds(al(q * width, width), width), :]
        if k == 2:
            return upw_ref.at[:, pl.ds(al(q * hid, hid), hid)]
        return dnw_ref.at[pl.ds(al(q * hid, hid), hid), :]

    trio_in = (conv_ref, outer_ref, inner_ref)

    def trio_copies(dst, ys, sems):
        q = r * 2 + ys
        return [
            pltpu.make_async_copy(
                w.at[:, pl.ds(al(q * width, width), width)],
                dst.at[:, pl.ds(j * width, width)],
                sems.at[j],
            )
            for j, w in enumerate(trio_in)
        ]

    own_trio = trio_copies(place(0, z, y), y, local_sem)
    other_trio = trio_copies(stage, 1 - y, stage_sem)
    own_rest = [None] + [pltpu.make_async_copy(share(k, y), place(k, z, y), local_sem.at[2 + k]) for k in (1, 2, 3)]
    for copy in other_trio + own_trio + own_rest[1:]:
        copy.start()

    def near_copy(k):
        a = stage if k == 0 else share(k, 1 - y)
        return push(a, place(k, z, y), near_send.at[k], w_recv.at[k, z * 2 + y], beside)

    def hop(k, zs, ys, step, sems):
        p = zs * 2 + ys
        at = place(k, zs, ys)
        return push(at, at, sems.at[k, p], w_recv.at[k, p], (r, z + step, y, t))

    order = visit_order(far)

    def nth(j):
        zs = jnp.int32(order[0][j])
        for c in range(1, far):
            zs = jnp.where(z == c, order[c][j], zs)
        return zs

    def send_on(k, zs, ys):
        @pl.when(jnp.logical_and(zs <= z, z + 1 < far))
        def _():
            hop(k, zs, ys, 1, right_send).start()

        @pl.when(jnp.logical_and(zs >= z, z > 0))
        def _():
            hop(k, zs, ys, -1, left_send).start()

    def arrive_own(k):
        for copy in own_trio if k == 0 else [own_rest[k]]:
            copy.wait()
        send_on(k, z, y)

    def arrive_beside(k):
        push(place(k, z, 1 - y), place(k, z, 1 - y), near_send.at[k], w_recv.at[k, z * 2 + 1 - y], beside).wait_recv()
        send_on(k, z, 1 - y)

    def arrive(k, j):
        zs = nth(j)
        for ys in (y, 1 - y):
            push(
                place(k, zs, ys), place(k, zs, ys), near_send.at[k], w_recv.at[k, zs * 2 + ys], beside
            ).wait_recv()
            send_on(k, zs, ys)
        return zs

    def norm(values, gain_ref):
        inverse = lax.rsqrt(jnp.mean(values * values, axis=-1, keepdims=True) + eps)
        return (values * inverse * gain_ref[...]).astype(bf16)

    def slot(buf, c, core):
        return buf.at[pl.ds(al((c * 2 + core) * rows, rows), rows), :]

    def ag_copy(g, buf, i):
        at = slot(buf, m, t)
        where = sibling if i == 3 else chip(lax.rem(m + 1 + i, 4))
        return push(at, at, ag_send.at[g, i], ag_recv.at[g, m * 2 + t], where)

    def ag_relay(g, buf, i):
        c = lax.rem(m + 3 - i, 4)
        at = slot(buf, c, t)
        return push(at, at, ag_send.at[g, 4 + i], ag_recv.at[g, c * 2 + t], sibling)

    def ag_start(g, buf):
        for i in range(4):
            ag_copy(g, buf, i).start()

    def ag_wait(g, buf, c, core):
        at = slot(buf, c, core)
        push(at, at, ag_send.at[g, 0], ag_recv.at[g, c * 2 + core], sibling).wait_recv()

    def ag_finish(g, buf):
        for i in (0, 2, 1):
            ag_wait(g, buf, lax.rem(m + 3 - i, 4), t)
            ag_relay(g, buf, i).start()
        for i in range(4):
            ag_wait(g, buf, lax.rem(m + 3 - i, 4), 1 - t)

    for copy in other_trio:
        copy.wait()
    near_copy(0).start()
    near_copy(1).start()
    arrive_own(0)
    arrive_own(1)
    toks[pl.ds(al((m * 2 + t) * rows, rows), rows), :] = norm(tok_ref[...].astype(f32), mix_gain_ref)
    ag_start(0, toks)
    near_copy(2).start()
    near_copy(3).start()
    for k in (0, 1):
        arrive_beside(k)
    arrive_own(2)
    arrive_beside(2)
    for j in range(1, far):
        for k in (0, 1):
            arrive(k, j)
        if j == 1:
            ag_finish(0, toks)
    arrive(2, 1)
    arrive_own(3)
    arrive_beside(3)

    mix_cols = outb.shape[1]
    q = r * 2 + y
    taps = taps_ref[:, pl.ds(al(q * width, width), width)]

    def sib_copy(g, n, s, buf, land, lo, size):
        at = buf.at[pl.ds(al(s * seq + (1 - t) * rows, rows), rows), pl.ds(lo, size)]
        to = land.at[pl.ds(al(s * rows, rows), rows), pl.ds(lo, size)]
        return push(at, to, sib_send.at[n, s], sib_recv.at[n, s], sibling)

    def rs_copy(n, i, send, land, lo, size):
        at = send.at[i, :, pl.ds(lo, size)]
        return push(at, land.at[i, :, pl.ds(lo, size)], rs_send.at[n, i], rs_recv.at[n, i], chip(lax.rem(m + 1 + i, 4)))

    def rs_middle(g, n, buf, land, send, rland, lo, size):
        for i in range(4):
            s = lax.rem(m + 1 + i, 4)
            sib_copy(g, n, s, buf, land, lo, size).wait_recv()
            total = (
                buf[pl.ds(al(s * seq + t * rows, rows), rows), pl.ds(lo, size)].astype(f32)
                + land[pl.ds(al(s * rows, rows), rows), pl.ds(lo, size)].astype(f32)
            )
            send[i, :, pl.ds(lo, size)] = total.astype(bf16)
            if i < 3:
                rs_copy(n, i, send, rland, lo, size).start()

    def rs_total(n, send, rland, lo, size):
        total = send[3, :, pl.ds(lo, size)].astype(f32)
        for i in range(3):
            rs_copy(n, i, send, rland, lo, size).wait_recv()
            total = total + rland[i, :, pl.ds(lo, size)].astype(f32)
        return total

    @pl.loop(0, 4)
    def _(i):
        s = lax.rem(m + 1 + i, 4)
        x = toks[pl.ds(al(s * seq, seq), seq), :]
        proj = jnp.dot(x, trio[...], preferred_element_type=f32).astype(bf16).astype(f32)
        gated = proj[:, 2 * width :] * proj[:, :width]
        row = lax.broadcasted_iota(jnp.int32, gated.shape, 0)
        back1 = jnp.where(row < 1, 0.0, pltpu.roll(gated, 1, 0))
        back2 = jnp.where(row < 2, 0.0, pltpu.roll(gated, 2, 0))
        convolved = taps[0:1] * back2 + taps[1:2] * back1 + taps[2:3] * gated
        mixed = (proj[:, width : 2 * width] * convolved).astype(bf16)
        for lo in range(0, mix_cols, 1024):
            size = min(1024, mix_cols - lo)
            part[pl.ds(al(s * seq, seq), seq), pl.ds(lo, size)] = jnp.dot(
                mixed, outb[:, pl.ds(lo, size)], preferred_element_type=f32
            ).astype(bf16)
        sib_copy(0, 0, s, part, sib, 0, mix_cols).start()

    rs_middle(0, 0, part, sib, rsend, rrecv, 0, mix_cols)
    resid[...] = (tok_ref[...].astype(f32) + rs_total(0, rsend, rrecv, 0, mix_cols)).astype(bf16)
    toks_ff[pl.ds(al((m * 2 + t) * rows, rows), rows), :] = norm(resid[...].astype(f32), ff_gain_ref)
    ag_start(1, toks_ff)
    for j in range(2, far):
        arrive(2, j)
        if j == 2:
            ag_finish(1, toks_ff)
    if far < 3:
        ag_finish(1, toks_ff)

    @pl.loop(0, 4)
    def _(s):
        x = toks_ff[pl.ds(al(s * seq, seq), seq), :]
        half = hid // 2
        for lo in (0, half):
            act = jnp.dot(x, upb[:, pl.ds(lo, half)], preferred_element_type=f32)
            hidden[pl.ds(al(s * seq, seq), seq), pl.ds(lo, half)] = jnp.square(jnp.maximum(act, 0.0)).astype(bf16)

    group = 2 * cols

    def down(zs):
        lo = al(zs * group, group)

        @pl.loop(0, 4)
        def _(i):
            s = lax.rem(m + 1 + i, 4)
            part_ff[pl.ds(al(s * seq, seq), seq), pl.ds(lo, group)] = jnp.dot(
                hidden[pl.ds(al(s * seq, seq), seq), :], dnb[:, pl.ds(lo, group)], preferred_element_type=f32
            ).astype(bf16)
            sib_copy(1, 1 + zs, s, part_ff, sib_ff, lo, group).start()

        rs_middle(1, 1 + zs, part_ff, sib_ff, rsend_ff, rrecv_ff, lo, group)

    down(z)
    for j in range(1, far):
        down(arrive(3, j))
    for j in range(far):
        zs = nth(j)
        lo = al(zs * group, group)
        total = rs_total(1 + zs, rsend_ff, rrecv_ff, lo, group)
        o_ref[:, pl.ds(lo, group)] = (resid[:, pl.ds(lo, group)].astype(f32) + total).astype(bf16)

    for k in range(4):
        near_copy(k).wait_send()
        for zs in range(far):
            for ys in range(2):
                @pl.when(jnp.logical_and(zs <= z, z + 1 < far))
                def _():
                    hop(k, zs, ys, 1, right_send).wait_send()

                @pl.when(jnp.logical_and(zs >= z, z > 0))
                def _():
                    hop(k, zs, ys, -1, left_send).wait_send()
    for g, buf in ((0, toks), (1, toks_ff)):
        for i in range(4):
            ag_copy(g, buf, i).wait_send()
        for i in range(3):
            ag_relay(g, buf, i).wait_send()
    for s in range(4):
        sib_copy(0, 0, s, part, sib, 0, mix_cols).wait_send()
        for zs in range(far):
            sib_copy(1, 1 + zs, s, part_ff, sib_ff, zs * group, group).wait_send()
    for i in range(3):
        rs_copy(0, i, rsend, rrecv, 0, mix_cols).wait_send()
        for zs in range(far):
            rs_copy(1 + zs, i, rsend_ff, rrecv_ff, zs * group, group).wait_send()


def fused_layer(far, tokens, mix_gain, conv_in, outer, inner, taps, out_w, ff_gain, up_w, down_w):
    bf16 = jnp.bfloat16
    rows, feat = tokens.shape
    depth, cols = up_w.shape[0], down_w.shape[1]
    width, hid = conv_in.shape[1] // 4, up_w.shape[1] // 4
    whole = 8 * rows
    vmem = pl.BlockSpec(memory_space=pltpu.VMEM)
    hbm = pl.BlockSpec(memory_space=pl.ANY)
    dma = pltpu.SemaphoreType.DMA
    block = [
        pltpu.VMEM((whole, feat), bf16),
        pltpu.VMEM((4 * rows, feat), bf16),
        pltpu.VMEM((4, rows, feat), bf16),
        pltpu.VMEM((3, rows, feat), bf16),
    ]
    return pl.pallas_call(
        functools.partial(layer_kernel, far),
        out_shape=jax.ShapeDtypeStruct((rows, feat), bf16),
        in_specs=[vmem, vmem, hbm, hbm, hbm, vmem, hbm, vmem, hbm, hbm],
        out_specs=vmem,
        scratch_shapes=[
            pltpu.VMEM((far * 2 * depth, 3 * width), bf16),
            pltpu.VMEM((width, far * 2 * cols), bf16),
            pltpu.VMEM((far * 2 * depth, hid), bf16),
            pltpu.VMEM((hid, far * 2 * cols), bf16),
            pltpu.VMEM((depth, 3 * width), bf16),
            pltpu.VMEM((whole, feat), bf16),
            pltpu.VMEM((whole, feat), bf16),
            *block,
            *block,
            pltpu.VMEM((whole, hid), bf16),
            pltpu.VMEM((rows, feat), bf16),
            dma((6,)),
            dma((3,)),
            dma((4,)),
            dma((4, far * 2)),
            dma((4, far * 2)),
            dma((4, far * 2)),
            dma((2, 7)),
            dma((2, 8)),
            dma((1 + far, 4)),
            dma((1 + far, 4)),
            dma((1 + far, 3)),
            dma((1 + far, 3)),
        ],
        compiler_params=pltpu.CompilerParams(has_side_effects=True, vmem_limit_bytes=60 * 2**20),
    )(tokens, mix_gain[None], conv_in, outer, inner, taps, out_w, ff_gain[None], up_w, down_w)


def solution(mesh):
    rep, fs, tp = (mesh.shape[name] for name in ("rep", "fs", "tp"))
    near = 2 if fs % 2 == 0 else 1
    mesh4 = Mesh(mesh.devices.reshape(rep, fs // near, near, tp), ("rep", "far", "near", "tp"))
    fs_axes = ("far", "near")
    rows = P(("rep", "far", "near", "tp"), None)
    in_specs = (
        rows,
        P(),
        P(fs_axes, "tp"),
        P(fs_axes, "tp"),
        P(fs_axes, "tp"),
        P(None, "tp"),
        P("tp", fs_axes),
        P(),
        P(fs_axes, "tp"),
        P("tp", fs_axes),
    )

    def body(*args):
        if rep == 2 and near == 2 and tp == 2:
            return fused_layer(fs // near, *args)
        return on_device(rep, near, tp, *args)

    return jax.shard_map(body, mesh=mesh4, in_specs=in_specs, out_specs=rows, check_vma=False)
```

profile of v0, /device:TPU:0, one launch (start us, length us, event | category | flops | bytes accessed | tf_op | source)
XLA Modules:
  0.0 215.6 jit_solution(2270000050107896308)
XLA Ops:
  0.0 213.7 %shard_map.100 = bf16[128,2048]{1,0:T(8,128)(2,1)} custom-call(bf16[128,2048]{1,0:T(8,128)(2,1)} %tok_ref.1, f32[1,2048]{1,0:T(1,128)} %bitcast.2, bf16[256,512]{1,0:T(8,128)(2,1)} %conv_ref.1, bf16[256,512]{1,0:T(8,128)(2,1)} %outer_ref.1, bf16[256,512]{1,0:T(8,128)(2,1)} %inner_ref.1, f32[3,512]{1,0:T(4,128)} %taps_ref.1, bf16[512,256]{1,0:T(8,128)(2,1)} %outw_ref.1, ...), custom_call_target="tpu_custom_call" | custom-call | tf_op jit(solution)/shard_map/pallas_call | solution.py:384
  213.7 1.9 copy.12
where the time goes:
time: 216 us
  Pallas kernels  214 us (99%)
    pallas_call x1, Pallas kernels, fused_layer(): pl.pallas_call(functools.partial(layer_kernel, far), out_shape=jax.ShapeD...  214 us

commit v1 on v0

v1 whole, which is shorter than its diff:
```python
import functools

import jax
import jax.numpy as jnp
from jax import lax
from jax.experimental import pallas as pl
from jax.experimental.pallas import tpu as pltpu
from jax.sharding import Mesh, PartitionSpec as P

eps = 1e-06


def rms_scale(values, gain):
    widened = values.astype(jnp.float32)
    inverse = lax.rsqrt(jnp.mean(widened * widened, axis=-1, keepdims=True) + eps)
    return (widened * inverse * gain).astype(jnp.bfloat16)


GROUP = ("rep", "near", "tp")


def gather_rows(block, near):
    rows, width = block.shape[0], block.shape[1] // near
    if near > 1:
        block = lax.all_to_all(
            block.reshape(rows, near, width).transpose(1, 0, 2), "near", 0, 0, tiled=True
        ).reshape(near * rows, width)
    return lax.all_gather(block, "far", axis=0, tiled=True)


def own_part(block, axis, rep):
    size = block.shape[axis] // rep
    return lax.dynamic_slice_in_dim(block, lax.axis_index("rep") * size, size, axis)


def on_device(rep, near, tp, tokens, mix_gain, conv_in, outer, inner, taps, out_w, ff_gain, up_w, down_w):
    seq_rows = tokens.shape[0] * tp
    depth = up_w.shape[0]
    parts = [own_part(w, 1, rep) for w in (conv_in, outer, inner)]
    width = parts[0].shape[1] // near
    trio = jnp.concatenate([p.reshape(depth, near, width) for p in parts], 2).reshape(depth, -1)
    trio = gather_rows(trio, near)
    out_part = own_part(out_w, 0, rep)
    out_part = out_part.reshape(near, width, -1).transpose(1, 0, 2).reshape(width, -1)
    out_full = gather_rows(out_part, near).reshape(-1, width, out_w.shape[1])
    up_full = gather_rows(own_part(up_w, 1, rep), near)
    down_part = own_part(down_w, 0, rep)
    hid = down_part.shape[0] // near
    down_part = down_part.reshape(near, hid, -1).transpose(1, 0, 2).reshape(hid, -1)
    down_full = gather_rows(down_part, near).reshape(-1, hid, down_w.shape[1])

    taps = own_part(taps, 1, rep)
    taps = lax.dynamic_slice_in_dim(taps, lax.axis_index("near") * width, width, 1)

    normed = lax.all_gather(rms_scale(tokens, mix_gain), GROUP, axis=0, tiled=True)
    proj = jnp.dot(normed, trio, preferred_element_type=jnp.float32).astype(jnp.bfloat16)
    proj = proj.astype(jnp.float32).reshape(-1, seq_rows, 3 * width)
    gated = proj[..., 2 * width :] * proj[..., :width]
    padded = jnp.pad(gated, ((0, 0), (2, 0), (0, 0)))
    convolved = sum(taps[k] * padded[:, k : seq_rows + k] for k in range(3))
    mixed = (proj[..., width : 2 * width] * convolved).astype(jnp.bfloat16)
    mixed = mixed.reshape(-1, width)

    def project(lefts, rights):
        whole = rights.transpose(1, 0, 2).reshape(lefts.shape[1], -1)
        partial = jnp.dot(lefts, whole, preferred_element_type=jnp.float32)
        return lax.psum_scatter(
            partial.astype(jnp.bfloat16), GROUP, scatter_dimension=0, tiled=True
        ).astype(jnp.float32)

    resid = (tokens.astype(jnp.float32) + project(mixed, out_full)).astype(jnp.bfloat16)
    normed_ff = lax.all_gather(rms_scale(resid, ff_gain), GROUP, axis=0, tiled=True)
    preact = jnp.dot(normed_ff, up_full, preferred_element_type=jnp.float32)
    hidden = jnp.square(jax.nn.relu(preact)).astype(jnp.bfloat16)
    return (resid.astype(jnp.float32) + project(hidden, down_full)).astype(jnp.bfloat16)


def layer_kernel(
    far,
    tok_ref, mix_gain_ref, conv_ref, outer_ref, inner_ref, taps_ref, outw_ref, ff_gain_ref, upw_ref, dnw_ref,
    o_ref,
    trio, outb, upb, dnb, stage, toks, toks_ff,
    part, sib, xs, xr, zs_, zr, part_ff, sib_ff, xs_ff, xr_ff, zs_ff, zr_ff,
    hidden, resid,
    local_sem, stage_sem, w_send, y_send, w_recv,
    ag_send, ag_recv, sib_send, sib_recv, x_send, x_recv, z_send, z_recv,
):
    r, z, y, t = (lax.axis_index(name) for name in ("rep", "far", "near", "tp"))
    rows = tok_ref.shape[0]
    seq = 2 * rows
    width = trio.shape[1] // 3
    depth, hid = upw_ref.shape[0], upb.shape[1]
    cols = dnw_ref.shape[1]
    group = 2 * cols
    bf16, f32 = jnp.bfloat16, jnp.float32

    pair, e = lax.div(z, 2), lax.rem(z, 2)
    edge = lax.rem(pair + e + 1, 2)
    zp = z + 1 - 2 * e
    zm = far - 1 - z
    zd = far - 1 - zp
    line = (z, zp, zm, zd)
    c = r * 2 + e
    cx, cz, cd = (1 - r) * 2 + e, r * 2 + 1 - e, (1 - r) * 2 + 1 - e
    q_own, q_other = r * 2 + edge, r * 2 + 1 - edge

    sibling = (r, z, y, 1 - t)
    beside = (r, z, 1 - y, t)
    across = (1 - r, z, y, t)
    partner = (r, zp, y, t)

    def al(v, n):
        return pl.multiple_of(v, n)

    def push(a, b, s, q, where):
        return pltpu.make_async_remote_copy(
            src_ref=a, dst_ref=b, send_sem=s, recv_sem=q, device_id=where, device_id_type=pl.DeviceIdType.MESH
        )

    def place(k, zs, ys):
        p = zs * 2 + ys
        if k == 0:
            return trio.at[pl.ds(al(p * depth, depth), depth), :]
        if k == 1:
            return outb.at[:, pl.ds(al(p * cols, cols), cols)]
        if k == 2:
            return upb.at[pl.ds(al(p * depth, depth), depth), :]
        return dnb.at[:, pl.ds(al(p * cols, cols), cols)]

    def share(k, q):
        if k == 1:
            return outw_ref.at[pl.ds(al(q * width, width), width), :]
        if k == 2:
            return upw_ref.at[:, pl.ds(al(q * hid, hid), hid)]
        return dnw_ref.at[pl.ds(al(q * hid, hid), hid), :]

    def trio_copies(dst, q, sems):
        return [
            pltpu.make_async_copy(
                w.at[:, pl.ds(al(q * width, width), width)],
                dst.at[:, pl.ds(j * width, width)],
                sems.at[j],
            )
            for j, w in enumerate((conv_ref, outer_ref, inner_ref))
        ]

    own_trio = trio_copies(place(0, z, y), q_own, local_sem)
    other_trio = trio_copies(stage, q_other, stage_sem)
    own_rest = [None] + [
        pltpu.make_async_copy(share(k, q_own), place(k, z, y), local_sem.at[2 + k]) for k in (1, 2, 3)
    ]

    def own_src(k):
        return place(0, z, y) if k == 0 else share(k, q_own)

    def other_src(k):
        return stage if k == 0 else share(k, q_other)

    def w_copy(k, i):
        a = own_src(k) if i == 1 else other_src(k)
        return push(
            a, place(k, z, y), w_send.at[k, i], w_recv.at[k, z * 2 + y], (r, (zp, zm, zd)[i], y, t)
        )

    def y_copy(k, j):
        at = place(k, line[j], y)
        a = own_src(k) if j == 0 else at
        return push(a, at, y_send.at[k, j], w_recv.at[k, line[j] * 2 + y], beside)

    def w_start(k):
        for i in range(3):
            w_copy(k, i).start()

    def landed(k, j, ys):
        at = place(k, line[j], ys)
        push(at, at, y_send.at[k, j], w_recv.at[k, line[j] * 2 + ys], beside).wait_recv()

    def arrive(k, j):
        landed(k, j, y)
        y_copy(k, j).start()

    def norm(values, gain_ref):
        inverse = lax.rsqrt(jnp.mean(values * values, axis=-1, keepdims=True) + eps)
        return (values * inverse * gain_ref[...]).astype(bf16)

    def slot(buf, s, core):
        return buf.at[pl.ds(al((s * 2 + core) * rows, rows), rows), :]

    def ag_copy(g, buf, i):
        s, core, where = (
            (c, t, partner), (c, t, across), (c, t, sibling),
            (cz, t, across), (cz, t, sibling), (cx, t, sibling), (cd, t, sibling),
        )[i]
        at = slot(buf, s, core)
        return push(at, at, ag_send.at[g, i], ag_recv.at[g, s * 2 + core], where)

    def ag_wait(g, buf, s, core):
        at = slot(buf, s, core)
        push(at, at, ag_send.at[g, 0], ag_recv.at[g, s * 2 + core], sibling).wait_recv()

    def ag_start(g, buf):
        for i in range(3):
            ag_copy(g, buf, i).start()

    def ag_relay(g, buf, s, sends):
        ag_wait(g, buf, s, t)
        for i in sends:
            ag_copy(g, buf, i).start()

    def sib_copy(n, s, buf, land, lo, size):
        at = buf.at[pl.ds(al(s * seq + (1 - t) * rows, rows), rows), pl.ds(lo, size)]
        to = land.at[pl.ds(al(s * rows, rows), rows), pl.ds(lo, size)]
        return push(at, to, sib_send.at[n, s], sib_recv.at[n, s], sibling)

    def x_copy(n, j, send, land, lo, size):
        return push(
            send.at[j, :, pl.ds(lo, size)], land.at[j, :, pl.ds(lo, size)], x_send.at[n, j], x_recv.at[n, j], across
        )

    def z_copy(n, send, land, lo, size):
        return push(send.at[:, pl.ds(lo, size)], land.at[:, pl.ds(lo, size)], z_send.at[n], z_recv.at[n], partner)

    def both(s, buf, land, lo, size):
        return (
            buf[pl.ds(al(s * seq + t * rows, rows), rows), pl.ds(lo, size)].astype(f32)
            + land[pl.ds(al(s * rows, rows), rows), pl.ds(lo, size)].astype(f32)
        )

    def reduce_x(n, buf, land, send, xland, lo, size):
        for j, s in ((0, cd), (1, cx)):
            send[j, :, pl.ds(lo, size)] = both(s, buf, land, lo, size).astype(bf16)
            x_copy(n, j, send, xland, lo, size).start()

    def reduce_z(n, buf, land, send, xland, zsend, zland, lo, size):
        x_copy(n, 0, send, xland, lo, size).wait_recv()
        total = both(cz, buf, land, lo, size) + xland[0, :, pl.ds(lo, size)].astype(f32)
        zsend[:, pl.ds(lo, size)] = total.astype(bf16)
        z_copy(n, zsend, zland, lo, size).start()

    def reduce_end(n, buf, land, send, xland, zsend, zland, lo, size):
        x_copy(n, 1, send, xland, lo, size).wait_recv()
        z_copy(n, zsend, zland, lo, size).wait_recv()
        return (
            both(c, buf, land, lo, size)
            + xland[1, :, pl.ds(lo, size)].astype(f32)
            + zland[:, pl.ds(lo, size)].astype(f32)
        )

    def seq_at(i):
        rr = lax.rem(r + 1 + lax.div(i, 2), 2)
        ee = lax.rem(e + 1 + lax.rem(i, 2), 2)
        return rr * 2 + ee

    for copy in own_trio + other_trio + own_rest[1:]:
        copy.start()
    slot(toks, c, t)[...] = norm(tok_ref[...].astype(f32), mix_gain_ref)
    ag_start(0, toks)
    for copy in own_trio + other_trio:
        copy.wait()
    for k in (0, 1):
        w_start(k)
        y_copy(k, 0).start()
    w_start(2)
    ag_relay(0, toks, cz, (3, 4))
    ag_relay(0, toks, cx, (5,))
    for k in (0, 1):
        arrive(k, 1)
    y_copy(2, 0).start()
    for j in (2, 3):
        for k in (0, 1):
            arrive(k, j)
    ag_relay(0, toks, cd, (6,))
    for s in (c, cx, cz, cd):
        ag_wait(0, toks, s, 1 - t)
    own_rest[1].wait()
    for j in range(4):
        for k in (0, 1):
            landed(k, j, 1 - y)

    mix_cols = outb.shape[1]
    taps = taps_ref[:, pl.ds(al(q_own * width, width), width)]

    @pl.loop(0, 4)
    def _(i):
        s = seq_at(i)
        x = toks[pl.ds(al(s * seq, seq), seq), :]
        proj = jnp.dot(x, trio[...], preferred_element_type=f32).astype(bf16).astype(f32)
        gated = proj[:, 2 * width :] * proj[:, :width]
        row = lax.broadcasted_iota(jnp.int32, gated.shape, 0)
        back1 = jnp.where(row < 1, 0.0, pltpu.roll(gated, 1, 0))
        back2 = jnp.where(row < 2, 0.0, pltpu.roll(gated, 2, 0))
        convolved = taps[0:1] * back2 + taps[1:2] * back1 + taps[2:3] * gated
        mixed = (proj[:, width : 2 * width] * convolved).astype(bf16)
        for lo in range(0, mix_cols, 1024):
            size = min(1024, mix_cols - lo)
            part[pl.ds(al(s * seq, seq), seq), pl.ds(lo, size)] = jnp.dot(
                mixed, outb[:, pl.ds(lo, size)], preferred_element_type=f32
            ).astype(bf16)
        sib_copy(0, s, part, sib, 0, mix_cols).start()

    mixer = (part, sib, xs, xr)
    for s in (cd, cx):
        sib_copy(0, s, part, sib, 0, mix_cols).wait_recv()
    for g in range(far):
        reduce_x(g, *mixer, g * group, group)
    for s in (cz, c):
        sib_copy(0, s, part, sib, 0, mix_cols).wait_recv()
    for g in range(far):
        reduce_z(g, *mixer, zs_, zr, g * group, group)
        if g == 2:
            arrive(2, 1)
    for g in range(far):
        at = pl.ds(g * group, group)
        total = reduce_end(g, *mixer, zs_, zr, g * group, group)
        resid[:, at] = (tok_ref[:, at].astype(f32) + total).astype(bf16)
    slot(toks_ff, c, t)[...] = norm(resid[...].astype(f32), ff_gain_ref)
    ag_start(1, toks_ff)
    w_start(3)
    for j in (2, 3):
        arrive(2, j)
    y_copy(3, 0).start()
    ag_relay(1, toks_ff, cz, (3, 4))
    ag_relay(1, toks_ff, cx, (5,))
    own_rest[2].wait()
    for j in range(4):
        landed(2, j, 1 - y)
    ag_relay(1, toks_ff, cd, (6,))
    for s in (c, cx, cz, cd):
        ag_wait(1, toks_ff, s, 1 - t)

    @pl.loop(0, 4)
    def _(s):
        x = toks_ff[pl.ds(al(s * seq, seq), seq), :]
        half = hid // 2
        for lo in (0, half):
            act = jnp.dot(x, upb[:, pl.ds(lo, half)], preferred_element_type=f32)
            hidden[pl.ds(al(s * seq, seq), seq), pl.ds(lo, half)] = jnp.square(jnp.maximum(act, 0.0)).astype(bf16)

    ff = (part_ff, sib_ff, xs_ff, xr_ff)

    def down(j):
        zs = line[j]
        lo = al(zs * group, group)

        @pl.loop(0, 4)
        def _(i):
            s = seq_at(i)
            part_ff[pl.ds(al(s * seq, seq), seq), pl.ds(lo, group)] = jnp.dot(
                hidden[pl.ds(al(s * seq, seq), seq), :], dnb[:, pl.ds(lo, group)], preferred_element_type=f32
            ).astype(bf16)
            sib_copy(1 + zs, s, part_ff, sib_ff, lo, group).start()

        for s in (cd, cx):
            sib_copy(1 + zs, s, part_ff, sib_ff, lo, group).wait_recv()
        reduce_x(far + zs, *ff, lo, group)
        for s in (cz, c):
            sib_copy(1 + zs, s, part_ff, sib_ff, lo, group).wait_recv()

    def finish(j):
        zs = line[j]
        lo = al(zs * group, group)
        reduce_z(far + zs, *ff, zs_ff, zr_ff, lo, group)

    own_rest[3].wait()
    landed(3, 0, 1 - y)
    down(0)
    for j in range(1, 4):
        arrive(3, j)
        finish(j - 1)
        landed(3, j, 1 - y)
        down(j)
    finish(3)
    for j in range(4):
        zs = line[j]
        lo = al(zs * group, group)
        total = reduce_end(far + zs, *ff, zs_ff, zr_ff, lo, group)
        o_ref[:, pl.ds(lo, group)] = (resid[:, pl.ds(lo, group)].astype(f32) + total).astype(bf16)

    for k in range(4):
        for i in range(3):
            w_copy(k, i).wait_send()
        for j in range(4):
            y_copy(k, j).wait_send()
    for g, buf in ((0, toks), (1, toks_ff)):
        for i in range(7):
            ag_copy(g, buf, i).wait_send()
    for s in range(4):
        sib_copy(0, s, part, sib, 0, mix_cols).wait_send()
        for n in range(far):
            sib_copy(1 + n, s, part_ff, sib_ff, n * group, group).wait_send()
    for n in range(far):
        lo = n * group
        for j in range(2):
            x_copy(n, j, xs, xr, lo, group).wait_send()
            x_copy(far + n, j, xs_ff, xr_ff, lo, group).wait_send()
        z_copy(n, zs_, zr, lo, group).wait_send()
        z_copy(far + n, zs_ff, zr_ff, lo, group).wait_send()


def fused_layer(far, tokens, mix_gain, conv_in, outer, inner, taps, out_w, ff_gain, up_w, down_w):
    bf16 = jnp.bfloat16
    rows, feat = tokens.shape
    depth, cols = up_w.shape[0], down_w.shape[1]
    width, hid = conv_in.shape[1] // 4, up_w.shape[1] // 4
    whole = 8 * rows
    vmem = pl.BlockSpec(memory_space=pltpu.VMEM)
    hbm = pl.BlockSpec(memory_space=pl.ANY)
    dma = pltpu.SemaphoreType.DMA
    block = [
        pltpu.VMEM((whole, feat), bf16),
        pltpu.VMEM((4 * rows, feat), bf16),
        pltpu.VMEM((2, rows, feat), bf16),
        pltpu.VMEM((2, rows, feat), bf16),
        pltpu.VMEM((rows, feat), bf16),
        pltpu.VMEM((rows, feat), bf16),
    ]
    return pl.pallas_call(
        functools.partial(layer_kernel, far),
        out_shape=jax.ShapeDtypeStruct((rows, feat), bf16),
        in_specs=[vmem, vmem, hbm, hbm, hbm, vmem, hbm, vmem, hbm, hbm],
        out_specs=vmem,
        scratch_shapes=[
            pltpu.VMEM((far * 2 * depth, 3 * width), bf16),
            pltpu.VMEM((width, far * 2 * cols), bf16),
            pltpu.VMEM((far * 2 * depth, hid), bf16),
            pltpu.VMEM((hid, far * 2 * cols), bf16),
            pltpu.VMEM((depth, 3 * width), bf16),
            pltpu.VMEM((whole, feat), bf16),
            pltpu.VMEM((whole, feat), bf16),
            *block,
            *block,
            pltpu.VMEM((whole, hid), bf16),
            pltpu.VMEM((rows, feat), bf16),
            dma((6,)),
            dma((3,)),
            dma((4, 3)),
            dma((4, 4)),
            dma((4, far * 2)),
            dma((2, 7)),
            dma((2, 8)),
            dma((1 + far, 4)),
            dma((1 + far, 4)),
            dma((2 * far, 2)),
            dma((2 * far, 2)),
            dma((2 * far,)),
            dma((2 * far,)),
        ],
        compiler_params=pltpu.CompilerParams(has_side_effects=True, vmem_limit_bytes=60 * 2**20),
    )(tokens, mix_gain[None], conv_in, outer, inner, taps, out_w, ff_gain[None], up_w, down_w)


def solution(mesh):
    rep, fs, tp = (mesh.shape[name] for name in ("rep", "fs", "tp"))
    near = 2 if fs % 2 == 0 else 1
    mesh4 = Mesh(mesh.devices.reshape(rep, fs // near, near, tp), ("rep", "far", "near", "tp"))
    fs_axes = ("far", "near")
    rows = P(("rep", "far", "near", "tp"), None)
    in_specs = (
        rows,
        P(),
        P(fs_axes, "tp"),
        P(fs_axes, "tp"),
        P(fs_axes, "tp"),
        P(None, "tp"),
        P("tp", fs_axes),
        P(),
        P(fs_axes, "tp"),
        P("tp", fs_axes),
    )

    def body(*args):
        if rep == 2 and near == 2 and tp == 2 and fs == 8:
            return fused_layer(fs // near, *args)
        return on_device(rep, near, tp, *args)

    return jax.shard_map(body, mesh=mesh4, in_specs=in_specs, out_specs=rows, check_vma=False)
```

time: 216 us -> 211 us (0.977)
  Pallas kernels: 214 us -> 209 us
    pallas_call x1, Pallas kernels: 214 us -> 209 us  [fused_layer(): pl.pallas_call(functools.partial(layer_kernel, far), out_shape=jax.ShapeD...]
where the time goes in v1:
time: 211 us
  Pallas kernels  209 us (99%)
    pallas_call x1, Pallas kernels, fused_layer(): pl.pallas_call(functools.partial(layer_kernel, far), out_shape=jax.ShapeD...  209 us

profile of v1, /device:TPU:0, one launch (start us, length us, event | category | flops | bytes accessed | tf_op | source)
XLA Modules:
  0.0 210.6 jit_solution(3496148101054966019)
XLA Ops:
  0.0 208.7 %shard_map.100 = bf16[128,2048]{1,0:T(8,128)(2,1)} custom-call(bf16[128,2048]{1,0:T(8,128)(2,1)} %tok_ref.1, f32[1,2048]{1,0:T(1,128)} %bitcast.2, bf16[256,512]{1,0:T(8,128)(2,1)} %conv_ref.1, bf16[256,512]{1,0:T(8,128)(2,1)} %outer_ref.1, bf16[256,512]{1,0:T(8,128)(2,1)} %inner_ref.1, f32[3,512]{1,0:T(4,128)} %taps_ref.1, bf16[512,256]{1,0:T(8,128)(2,1)} %outw_ref.1, ...), custom_call_target="tpu_custom_call" | custom-call | tf_op jit(solution)/shard_map/pallas_call | solution.py:417
  208.7 1.9 copy.12

commit v2 on v1

--- a/solution.py
+++ b/solution.py
@@ -75,15 +75,19 @@
     return (resid.astype(jnp.float32) + project(hidden, down_full)).astype(jnp.bfloat16)
 
 
+def visit_order(far):
+    return [sorted(range(far), key=lambda s: (abs(s - z), s)) for z in range(far)]
+
+
 def layer_kernel(
     far,
     tok_ref, mix_gain_ref, conv_ref, outer_ref, inner_ref, taps_ref, outw_ref, ff_gain_ref, upw_ref, dnw_ref,
     o_ref,
     trio, outb, upb, dnb, stage, toks, toks_ff,
-    part, sib, xs, xr, zs_, zr, part_ff, sib_ff, xs_ff, xr_ff, zs_ff, zr_ff,
+    part, sib, xs, xr, ps, pr, part_ff, sib_ff, xs_ff, xr_ff, ps_ff, pr_ff,
     hidden, resid,
-    local_sem, stage_sem, w_send, y_send, w_recv,
-    ag_send, ag_recv, sib_send, sib_recv, x_send, x_recv, z_send, z_recv,
+    local_sem, stage_sem, near_send, right_send, left_send, w_send, y_send, w_recv,
+    ag_send, ag_recv, sib_send, sib_recv, x_send, x_recv, p_send, p_recv,
 ):
     r, z, y, t = (lax.axis_index(name) for name in ("rep", "far", "near", "tp"))
     rows = tok_ref.shape[0]
@@ -91,23 +95,26 @@
     width = trio.shape[1] // 3
     depth, hid = upw_ref.shape[0], upb.shape[1]
     cols = dnw_ref.shape[1]
-    group = 2 * cols
+    group, strip = 2 * cols, cols // 2
     bf16, f32 = jnp.bfloat16, jnp.float32
 
-    pair, e = lax.div(z, 2), lax.rem(z, 2)
-    edge = lax.rem(pair + e + 1, 2)
-    zp = z + 1 - 2 * e
+    pair, half_z = lax.div(z, 2), lax.rem(z, 2)
+    edge = lax.rem(pair + half_z + 1, 2)
+    zp = z + 1 - 2 * half_z
     zm = far - 1 - z
     zd = far - 1 - zp
     line = (z, zp, zm, zd)
-    c = r * 2 + e
-    cx, cz, cd = (1 - r) * 2 + e, r * 2 + 1 - e, (1 - r) * 2 + 1 - e
+    side = (y, half_z)
+    own, cross, pal, diag = (
+        [rr * 2 + ee for ee in ends]
+        for rr, ends in ((r, side), (1 - r, side), (r, (1 - y, 1 - half_z)), (1 - r, (1 - y, 1 - half_z)))
+    )
     q_own, q_other = r * 2 + edge, r * 2 + 1 - edge
 
     sibling = (r, z, y, 1 - t)
     beside = (r, z, 1 - y, t)
     across = (1 - r, z, y, t)
-    partner = (r, zp, y, t)
+    partner = (beside, (r, zp, y, t))
 
     def al(v, n):
         return pl.multiple_of(v, n)
@@ -125,14 +132,15 @@
             return outb.at[:, pl.ds(al(p * cols, cols), cols)]
         if k == 2:
             return upb.at[pl.ds(al(p * depth, depth), depth), :]
-        return dnb.at[:, pl.ds(al(p * cols, cols), cols)]
+        lo = ((zs * 2 + k - 3) * 2 + ys) * strip
+        return dnb.at[:, pl.ds(al(lo, strip), strip)]
 
     def share(k, q):
         if k == 1:
             return outw_ref.at[pl.ds(al(q * width, width), width), :]
         if k == 2:
             return upw_ref.at[:, pl.ds(al(q * hid, hid), hid)]
-        return dnw_ref.at[pl.ds(al(q * hid, hid), hid), :]
+        return dnw_ref.at[pl.ds(al(q * hid, hid), hid), pl.ds((k - 3) * strip, strip)]
 
     def trio_copies(dst, q, sems):
         return [
@@ -144,36 +152,63 @@
             for j, w in enumerate((conv_ref, outer_ref, inner_ref))
         ]
 
-    own_trio = trio_copies(place(0, z, y), q_own, local_sem)
-    other_trio = trio_copies(stage, q_other, stage_sem)
+    own_trio = trio_copies(place(0, z, y), r * 2 + y, local_sem)
+    other_trio = trio_copies(stage, r * 2 + 1 - y, stage_sem)
     own_rest = [None] + [
-        pltpu.make_async_copy(share(k, q_own), place(k, z, y), local_sem.at[2 + k]) for k in (1, 2, 3)
+        pltpu.make_async_copy(share(k, r * 2 + y if k == 1 else q_own), place(k, z, y), local_sem.at[2 + k])
+        for k in (1, 2, 3, 4)
     ]
 
-    def own_src(k):
-        return place(0, z, y) if k == 0 else share(k, q_own)
-
-    def other_src(k):
-        return stage if k == 0 else share(k, q_other)
+    def near_copy(k):
+        a = stage if k == 0 else share(k, r * 2 + 1 - y)
+        return push(a, place(k, z, y), near_send.at[k], w_recv.at[k, z * 2 + y], beside)
+
+    def hop(k, zs, ys, step, sems):
+        p = zs * 2 + ys
+        at = place(k, zs, ys)
+        return push(at, at, sems.at[k, p], w_recv.at[k, p], (r, z + step, y, t))
+
+    order = visit_order(far)
+
+    def nth(j):
+        zs = jnp.int32(order[0][j])
+        for c in range(1, far):
+            zs = jnp.where(z == c, order[c][j], zs)
+        return zs
+
+    def send_on(k, zs, ys):
+        @pl.when(jnp.logical_and(zs <= z, z + 1 < far))
+        def _():
+            hop(k, zs, ys, 1, right_send).start()
+
+        @pl.when(jnp.logical_and(zs >= z, z > 0))
+        def _():
+            hop(k, zs, ys, -1, left_send).start()
+
+    def mix_landed(k, zs, ys):
+        at = place(k, zs, ys)
+        push(at, at, near_send.at[k], w_recv.at[k, zs * 2 + ys], beside).wait_recv()
+        send_on(k, zs, ys)
 
     def w_copy(k, i):
-        a = own_src(k) if i == 1 else other_src(k)
+        a = share(k, q_own if i == 1 else q_other)
         return push(
-            a, place(k, z, y), w_send.at[k, i], w_recv.at[k, z * 2 + y], (r, (zp, zm, zd)[i], y, t)
+            a, place(k, z, y), w_send.at[k - 2, i], w_recv.at[k, z * 2 + y], (r, (zp, zm, zd)[i], y, t)
         )
+
+    def w_when(k, i, at_edge):
+        @pl.when(edge == at_edge)
+        def _():
+            w_copy(k, i).start()
 
     def y_copy(k, j):
         at = place(k, line[j], y)
-        a = own_src(k) if j == 0 else at
-        return push(a, at, y_send.at[k, j], w_recv.at[k, line[j] * 2 + y], beside)
-
-    def w_start(k):
-        for i in range(3):
-            w_copy(k, i).start()
+        a = share(k, q_own) if j == 0 else at
+        return push(a, at, y_send.at[k - 2, j], w_recv.at[k, line[j] * 2 + y], beside)
 
     def landed(k, j, ys):
         at = place(k, line[j], ys)
-        push(at, at, y_send.at[k, j], w_recv.at[k, line[j] * 2 + ys], beside).wait_recv()
+        push(at, at, y_send.at[k - 2, j], w_recv.at[k, line[j] * 2 + ys], beside).wait_recv()
 
     def arrive(k, j):
         landed(k, j, y)
@@ -188,8 +223,8 @@
 
     def ag_copy(g, buf, i):
         s, core, where = (
-            (c, t, partner), (c, t, across), (c, t, sibling),
-            (cz, t, across), (cz, t, sibling), (cx, t, sibling), (cd, t, sibling),
+            (own[g], t, partner[g]), (own[g], t, across), (own[g], t, sibling),
+            (pal[g], t, across), (pal[g], t, sibling), (cross[g], t, sibling), (diag[g], t, sibling),
         )[i]
         at = slot(buf, s, core)
         return push(at, at, ag_send.at[g, i], ag_recv.at[g, s * 2 + core], where)
@@ -217,8 +252,8 @@
             send.at[j, :, pl.ds(lo, size)], land.at[j, :, pl.ds(lo, size)], x_send.at[n, j], x_recv.at[n, j], across
         )
 
-    def z_copy(n, send, land, lo, size):
-        return push(send.at[:, pl.ds(lo, size)], land.at[:, pl.ds(lo, size)], z_send.at[n], z_recv.at[n], partner)
+    def p_copy(g, n, send, land, lo, size):
+        return push(send.at[:, pl.ds(lo, size)], land.at[:, pl.ds(lo, size)], p_send.at[n], p_recv.at[n], partner[g])
 
     def both(s, buf, land, lo, size):
         return (
@@ -226,63 +261,90 @@
             + land[pl.ds(al(s * rows, rows), rows), pl.ds(lo, size)].astype(f32)
         )
 
-    def reduce_x(n, buf, land, send, xland, lo, size):
-        for j, s in ((0, cd), (1, cx)):
+    mixer = (part, sib, xs, xr, ps, pr)
+    ff = (part_ff, sib_ff, xs_ff, xr_ff, ps_ff, pr_ff)
+
+    def reduce_x(g, n, lo, size):
+        buf, land, send, xland, _, _ = (mixer, ff)[g]
+        for j, s in ((0, diag[g]), (1, cross[g])):
             send[j, :, pl.ds(lo, size)] = both(s, buf, land, lo, size).astype(bf16)
             x_copy(n, j, send, xland, lo, size).start()
 
-    def reduce_z(n, buf, land, send, xland, zsend, zland, lo, size):
+    def reduce_p(g, n, lo, size):
+        buf, land, send, xland, psend, pland = (mixer, ff)[g]
         x_copy(n, 0, send, xland, lo, size).wait_recv()
-        total = both(cz, buf, land, lo, size) + xland[0, :, pl.ds(lo, size)].astype(f32)
-        zsend[:, pl.ds(lo, size)] = total.astype(bf16)
-        z_copy(n, zsend, zland, lo, size).start()
-
-    def reduce_end(n, buf, land, send, xland, zsend, zland, lo, size):
+        total = both(pal[g], buf, land, lo, size) + xland[0, :, pl.ds(lo, size)].astype(f32)
+        psend[:, pl.ds(lo, size)] = total.astype(bf16)
+        p_copy(g, n, psend, pland, lo, size).start()
+
+    def reduce_end(g, n, lo, size):
+        buf, land, send, xland, psend, pland = (mixer, ff)[g]
         x_copy(n, 1, send, xland, lo, size).wait_recv()
-        z_copy(n, zsend, zland, lo, size).wait_recv()
+        p_copy(g, n, psend, pland, lo, size).wait_recv()
         return (
-            both(c, buf, land, lo, size)
+            both(own[g], buf, land, lo, size)
             + xland[1, :, pl.ds(lo, size)].astype(f32)
-            + zland[:, pl.ds(lo, size)].astype(f32)
+            + pland[:, pl.ds(lo, size)].astype(f32)
         )
 
-    def seq_at(i):
+    def seq_at(g, i):
         rr = lax.rem(r + 1 + lax.div(i, 2), 2)
-        ee = lax.rem(e + 1 + lax.rem(i, 2), 2)
+        ee = lax.rem(side[g] + 1 + lax.rem(i, 2), 2)
         return rr * 2 + ee
 
-    for copy in own_trio + other_trio + own_rest[1:]:
+    barrier = pltpu.get_barrier_semaphore()
+    peers = (sibling, beside, across, partner[1], (r, zm, y, t), (r, zd, y, t))
+    for where in peers:
+        pl.semaphore_signal(barrier, inc=1, device_id=where, device_id_type=pl.DeviceIdType.MESH)
+    for copy in other_trio + own_trio + own_rest[1:]:
         copy.start()
-    slot(toks, c, t)[...] = norm(tok_ref[...].astype(f32), mix_gain_ref)
+    slot(toks, own[0], t)[...] = norm(tok_ref[...].astype(f32), mix_gain_ref)
+    pl.semaphore_wait(barrier, len(peers))
+    for copy in other_trio:
+        copy.wait()
+    near_copy(0).start()
+    near_copy(1).start()
+    for copy in own_trio:
+        copy.wait()
+    send_on(0, z, y)
+    own_rest[1].wait()
+    send_on(1, z, y)
     ag_start(0, toks)
-    for copy in own_trio + other_trio:
-        copy.wait()
     for k in (0, 1):
-        w_start(k)
+        mix_landed(k, z, 1 - y)
+    w_when(2, 0, 1)
+    for k in (0, 1):
+        for ys in (y, 1 - y):
+            mix_landed(k, nth(1), ys)
+    for k in (0, 1):
+        for ys in (y, 1 - y):
+            mix_landed(k, nth(2), ys)
+    ag_relay(0, toks, pal[0], (3, 4))
+    ag_relay(0, toks, cross[0], (5,))
+    y_copy(2, 0).start()
+    for k in (0, 1):
+        for ys in (y, 1 - y):
+            mix_landed(k, nth(3), ys)
+    for k in (3, 4):
         y_copy(k, 0).start()
-    w_start(2)
-    ag_relay(0, toks, cz, (3, 4))
-    ag_relay(0, toks, cx, (5,))
-    for k in (0, 1):
-        arrive(k, 1)
-    y_copy(2, 0).start()
-    for j in (2, 3):
-        for k in (0, 1):
-            arrive(k, j)
-    ag_relay(0, toks, cd, (6,))
-    for s in (c, cx, cz, cd):
+    w_when(2, 1, 0)
+    w_when(2, 2, 1)
+    ag_relay(0, toks, diag[0], (6,))
+    for s in (own[0], cross[0], pal[0], diag[0]):
         ag_wait(0, toks, s, 1 - t)
-    own_rest[1].wait()
-    for j in range(4):
-        for k in (0, 1):
-            landed(k, j, 1 - y)
+
+    w_when(2, 0, 0)
+
+    @pl.when(edge == 0)
+    def _():
+        arrive(2, 1)
 
     mix_cols = outb.shape[1]
-    taps = taps_ref[:, pl.ds(al(q_own * width, width), width)]
+    taps = taps_ref[:, pl.ds(al((r * 2 + y) * width, width), width)]
 
     @pl.loop(0, 4)
     def _(i):
-        s = seq_at(i)
+        s = seq_at(0, i)
         x = toks[pl.ds(al(s * seq, seq), seq), :]
         proj = jnp.dot(x, trio[...], preferred_element_type=f32).astype(bf16).astype(f32)
         gated = proj[:, 2 * width :] * proj[:, :width]
@@ -298,85 +360,120 @@
             ).astype(bf16)
         sib_copy(0, s, part, sib, 0, mix_cols).start()
 
-    mixer = (part, sib, xs, xr)
-    for s in (cd, cx):
+    for s in (diag[0], cross[0]):
         sib_copy(0, s, part, sib, 0, mix_cols).wait_recv()
-    for g in range(far):
-        reduce_x(g, *mixer, g * group, group)
-    for s in (cz, c):
+    for n in range(far):
+        reduce_x(0, n, n * group, group)
+    for s in (pal[0], own[0]):
         sib_copy(0, s, part, sib, 0, mix_cols).wait_recv()
-    for g in range(far):
-        reduce_z(g, *mixer, zs_, zr, g * group, group)
-        if g == 2:
-            arrive(2, 1)
-    for g in range(far):
-        at = pl.ds(g * group, group)
-        total = reduce_end(g, *mixer, zs_, zr, g * group, group)
+    for n in range(far):
+        reduce_p(0, n, n * group, group)
+        if n == 0:
+            w_when(2, 1, 1)
+            w_when(2, 2, 0)
+        if n == 2:
+            for k in (3, 4):
+                w_when(k, 0, 1)
+                w_when(k, 2, 1)
+
+    @pl.when(edge == 1)
+    def _():
+        arrive(2, 1)
+
+    for n in range(far):
+        at = pl.ds(n * group, group)
+        total = reduce_end(0, n, n * group, group)
         resid[:, at] = (tok_ref[:, at].astype(f32) + total).astype(bf16)
-    slot(toks_ff, c, t)[...] = norm(resid[...].astype(f32), ff_gain_ref)
+    slot(toks_ff, own[1], t)[...] = norm(resid[...].astype(f32), ff_gain_ref)
     ag_start(1, toks_ff)
-    w_start(3)
     for j in (2, 3):
         arrive(2, j)
-    y_copy(3, 0).start()
-    ag_relay(1, toks_ff, cz, (3, 4))
-    ag_relay(1, toks_ff, cx, (5,))
+    for k in (3, 4):
+        w_when(k, 1, 0)
+        w_when(k, 0, 0)
+    ag_relay(1, toks_ff, pal[1], (3, 4))
+    ag_relay(1, toks_ff, cross[1], (5,))
+    arrive(3, 1)
+    w_when(3, 1, 1)
+    w_when(3, 2, 0)
     own_rest[2].wait()
     for j in range(4):
         landed(2, j, 1 - y)
-    ag_relay(1, toks_ff, cd, (6,))
-    for s in (c, cx, cz, cd):
+
+    def up(i):
+        s = seq_at(1, 3 - i)
         ag_wait(1, toks_ff, s, 1 - t)
-
-    @pl.loop(0, 4)
-    def _(s):
         x = toks_ff[pl.ds(al(s * seq, seq), seq), :]
         half = hid // 2
         for lo in (0, half):
             act = jnp.dot(x, upb[:, pl.ds(lo, half)], preferred_element_type=f32)
             hidden[pl.ds(al(s * seq, seq), seq), pl.ds(lo, half)] = jnp.square(jnp.maximum(act, 0.0)).astype(bf16)
 
-    ff = (part_ff, sib_ff, xs_ff, xr_ff)
-
-    def down(j):
-        zs = line[j]
-        lo = al(zs * group, group)
+    pl.loop(0, 3)(up)
+    ag_relay(1, toks_ff, diag[1], (6,))
+    arrive(4, 1)
+    w_when(4, 1, 1)
+    w_when(4, 2, 0)
+    up(3)
+
+    def down(j, h):
+        m = line[j] * 2 + h
+        lo = al(m * cols, cols)
 
         @pl.loop(0, 4)
         def _(i):
-            s = seq_at(i)
-            part_ff[pl.ds(al(s * seq, seq), seq), pl.ds(lo, group)] = jnp.dot(
-                hidden[pl.ds(al(s * seq, seq), seq), :], dnb[:, pl.ds(lo, group)], preferred_element_type=f32
+            s = seq_at(1, i)
+            part_ff[pl.ds(al(s * seq, seq), seq), pl.ds(lo, cols)] = jnp.dot(
+                hidden[pl.ds(al(s * seq, seq), seq), :], dnb[:, pl.ds(lo, cols)], preferred_element_type=f32
             ).astype(bf16)
-            sib_copy(1 + zs, s, part_ff, sib_ff, lo, group).start()
-
-        for s in (cd, cx):
-            sib_copy(1 + zs, s, part_ff, sib_ff, lo, group).wait_recv()
-        reduce_x(far + zs, *ff, lo, group)
-        for s in (cz, c):
-            sib_copy(1 + zs, s, part_ff, sib_ff, lo, group).wait_recv()
-
-    def finish(j):
-        zs = line[j]
-        lo = al(zs * group, group)
-        reduce_z(far + zs, *ff, zs_ff, zr_ff, lo, group)
+            sib_copy(1 + m, s, part_ff, sib_ff, lo, cols).start()
+
+        for s in (diag[1], cross[1]):
+            sib_copy(1 + m, s, part_ff, sib_ff, lo, cols).wait_recv()
+        reduce_x(1, far + m, lo, cols)
+        for s in (pal[1], own[1]):
+            sib_copy(1 + m, s, part_ff, sib_ff, lo, cols).wait_recv()
+
+    def finish(j, h):
+        m = line[j] * 2 + h
+        reduce_p(1, far + m, al(m * cols, cols), cols)
+
+    def end(j, h):
+        m = line[j] * 2 + h
+        total = reduce_end(1, far + m, al(m * cols, cols), cols)
+        for ys in range(2):
+            at = pl.ds(al(line[j] * group + ys * cols + h * strip, strip), strip)
+            o_ref[:, at] = (resid[:, at].astype(f32) + total[:, ys * strip : (ys + 1) * strip]).astype(bf16)
 
     own_rest[3].wait()
-    landed(3, 0, 1 - y)
-    down(0)
-    for j in range(1, 4):
-        arrive(3, j)
-        finish(j - 1)
-        landed(3, j, 1 - y)
-        down(j)
-    finish(3)
-    for j in range(4):
-        zs = line[j]
-        lo = al(zs * group, group)
-        total = reduce_end(far + zs, *ff, zs_ff, zr_ff, lo, group)
-        o_ref[:, pl.ds(lo, group)] = (resid[:, pl.ds(lo, group)].astype(f32) + total).astype(bf16)
-
-    for k in range(4):
+    own_rest[4].wait()
+    steps = [(0, 0), (0, 1), (1, 0), (1, 1), (2, 0), (3, 0), (2, 1), (3, 1)]
+    ahead = {0: ((3, 2), (3, 3)), 2: ((4, 2),), 3: ((4, 3),)}
+    for n, (j, h) in enumerate(steps):
+        landed(3 + h, j, 1 - y)
+        down(j, h)
+        for block in ahead.get(n, ()):
+            arrive(*block)
+        if n > 0:
+            finish(*steps[n - 1])
+        if n > 2:
+            end(*steps[n - 3])
+    finish(*steps[-1])
+    for step in steps[-3:]:
+        end(*step)
+
+    for k in (0, 1):
+        near_copy(k).wait_send()
+        for zs in range(far):
+            for ys in range(2):
+                @pl.when(jnp.logical_and(zs <= z, z + 1 < far))
+                def _():
+                    hop(k, zs, ys, 1, right_send).wait_send()
+
+                @pl.when(jnp.logical_and(zs >= z, z > 0))
+                def _():
+                    hop(k, zs, ys, -1, left_send).wait_send()
+    for k in (2, 3, 4):
         for i in range(3):
             w_copy(k, i).wait_send()
         for j in range(4):
@@ -386,15 +483,18 @@
             ag_copy(g, buf, i).wait_send()
     for s in range(4):
         sib_copy(0, s, part, sib, 0, mix_cols).wait_send()
-        for n in range(far):
-            sib_copy(1 + n, s, part_ff, sib_ff, n * group, group).wait_send()
     for n in range(far):
         lo = n * group
         for j in range(2):
             x_copy(n, j, xs, xr, lo, group).wait_send()
-            x_copy(far + n, j, xs_ff, xr_ff, lo, group).wait_send()
-        z_copy(n, zs_, zr, lo, group).wait_send()
-        z_copy(far + n, zs_ff, zr_ff, lo, group).wait_send()
+        p_copy(0, n, ps, pr, lo, group).wait_send()
+    for m in range(2 * far):
+        lo = m * cols
+        for s in range(4):
+            sib_copy(1 + m, s, part_ff, sib_ff, lo, cols).wait_send()
+        for j in range(2):
+            x_copy(far + m, j, xs_ff, xr_ff, lo, cols).wait_send()
+        p_copy(1, far + m, ps_ff, pr_ff, lo, cols).wait_send()
 
 
 def fused_layer(far, tokens, mix_gain, conv_in, outer, inner, taps, out_w, ff_gain, up_w, down_w):
@@ -431,21 +531,25 @@
             *block,
             pltpu.VMEM((whole, hid), bf16),
             pltpu.VMEM((rows, feat), bf16),
-            dma((6,)),
+            dma((7,)),
             dma((3,)),
-            dma((4, 3)),
-            dma((4, 4)),
-            dma((4, far * 2)),
+            dma((2,)),
+            dma((2, far * 2)),
+            dma((2, far * 2)),
+            dma((3, 3)),
+            dma((3, 4)),
+            dma((5, far * 2)),
             dma((2, 7)),
             dma((2, 8)),
-            dma((1 + far, 4)),
-            dma((1 + far, 4)),
-            dma((2 * far, 2)),
-            dma((2 * far, 2)),
-            dma((2 * far,)),
-            dma((2 * far,)),
+            dma((1 + 2 * far, 4)),
+            dma((1 + 2 * far, 4)),
+            dma((3 * far, 2)),
+            dma((3 * far, 2)),
+            dma((3 * far,)),
+            dma((3 * far,)),
         ],
-        compiler_params=pltpu.CompilerParams(has_side_effects=True, vmem_limit_bytes=60 * 2**20),
+        compiler_params=pltpu.CompilerParams(
+            collective_id=0, has_side_effects=True, vmem_limit_bytes=60 * 2**20),
     )(tokens, mix_gain[None], conv_in, outer, inner, taps, out_w, ff_gain[None], up_w, down_w)
 
 

time: 211 us -> 160 us (0.76)
  Pallas kernels: 209 us -> 158 us
    pallas_call x1, Pallas kernels: 209 us -> 158 us  [fused_layer(): pl.pallas_call(functools.partial(layer_kernel, far), out_shape=jax.ShapeD...]
where the time goes in v2:
time: 160 us
  Pallas kernels  158 us (99%)
  local copies, waits for them, and re-layouts  1.88 us (1%)
    pallas_call x1, Pallas kernels, fused_layer(): pl.pallas_call(functools.partial(layer_kernel, far), out_shape=jax.ShapeD...  158 us

profile of v2, /device:TPU:0, one launch (start us, length us, event | category | flops | bytes accessed | tf_op | source)
XLA Modules:
  0.0 159.7 jit_solution(17488068137320466184)
XLA Ops:
  0.0 157.8 %shard_map.100 = bf16[128,2048]{1,0:T(8,128)(2,1)} custom-call(bf16[128,2048]{1,0:T(8,128)(2,1)} %tok_ref.1, f32[1,2048]{1,0:T(1,128)} %bitcast.2, bf16[256,512]{1,0:T(8,128)(2,1)} %conv_ref.1, bf16[256,512]{1,0:T(8,128)(2,1)} %outer_ref.1, bf16[256,512]{1,0:T(8,128)(2,1)} %inner_ref.1, f32[3,512]{1,0:T(4,128)} %taps_ref.1, bf16[512,256]{1,0:T(8,128)(2,1)} %outw_ref.1, ...), custom_call_target="tpu_custom_call" | custom-call | tf_op jit(solution)/shard_map/pallas_call | solution.py:517
  157.8 1.9 %copy.12 = bf16[128,2048]{1,0:T(8,128)(2,1)} copy(bf16[128,2048]{1,0:T(8,128)(2,1)} %shard_map.100) | data formatting | bytes 1048576

commit v3 on v2

--- a/solution.py
+++ b/solution.py
@@ -75,17 +75,49 @@
     return (resid.astype(jnp.float32) + project(hidden, down_full)).astype(jnp.bfloat16)
 
 
+SEND, OWN, TAKE = range(3)
+LATE = 6
+PLAN = (
+    {
+        2: ((OWN, 2, 0), (OWN, 3, 0), (OWN, 4, 0), (OWN, 5, 0),),
+        4: ((SEND, 2, 1), (SEND, 2, 0),),
+        5: ((TAKE, 2, 1),),
+        7: ((SEND, 2, 2),),
+        12: ((TAKE, 2, 2), (TAKE, 2, 3), (SEND, 3, 0), (SEND, 3, 1),),
+        13: ((SEND, 3, 2),),
+        14: ((TAKE, 3, 1), (SEND, 4, 0), (SEND, 5, 0), (SEND, 4, 1), (SEND, 5, 1), (SEND, 4, 2), (SEND, 5, 2),),
+        19: ((TAKE, 4, 1), (TAKE, 5, 1),),
+        20: ((TAKE, 3, 2), (TAKE, 3, 3),),
+        22: ((TAKE, 4, 2), (TAKE, 5, 2),),
+        23: ((TAKE, 4, 3), (TAKE, 5, 3),),
+    },
+    {
+        1: ((SEND, 2, 0),),
+        2: ((SEND, 2, 2), (OWN, 2, 0), (OWN, 3, 0), (OWN, 4, 0), (OWN, 5, 0),),
+        3: ((SEND, 3, 0), (SEND, 4, 0), (SEND, 5, 0),),
+        6: ((TAKE, 2, 1), (SEND, 2, 1),),
+        12: ((TAKE, 2, 2), (TAKE, 2, 3), (SEND, 3, 2),),
+        13: ((SEND, 3, 1),),
+        14: ((TAKE, 3, 1), (SEND, 4, 1), (SEND, 5, 1), (SEND, 4, 2), (SEND, 5, 2),),
+        19: ((TAKE, 4, 1), (TAKE, 5, 1),),
+        20: ((TAKE, 3, 2), (TAKE, 3, 3),),
+        22: ((TAKE, 4, 2), (TAKE, 5, 2),),
+        23: ((TAKE, 4, 3), (TAKE, 5, 3),),
+    },
+)
+
+
 def visit_order(far):
     return [sorted(range(far), key=lambda s: (abs(s - z), s)) for z in range(far)]
 
 
-def layer_kernel(
-    far,
+def chip_kernel(
+    far, edge,
     tok_ref, mix_gain_ref, conv_ref, outer_ref, inner_ref, taps_ref, outw_ref, ff_gain_ref, upw_ref, dnw_ref,
     o_ref,
     trio, outb, upb, dnb, stage, toks, toks_ff,
     part, sib, xs, xr, ps, pr, part_ff, sib_ff, xs_ff, xr_ff, ps_ff, pr_ff,
-    hidden, resid,
+    hidden, resid, result, out_sem,
     local_sem, stage_sem, near_send, right_send, left_send, w_send, y_send, w_recv,
     ag_send, ag_recv, sib_send, sib_recv, x_send, x_recv, p_send, p_recv,
 ):
@@ -93,13 +125,15 @@
     rows = tok_ref.shape[0]
     seq = 2 * rows
     width = trio.shape[1] // 3
-    depth, hid = upw_ref.shape[0], upb.shape[1]
+    depth = upw_ref.shape[0]
+    unit = upw_ref.shape[1] // 32
+    sizes = (8 * unit, 8 * unit)
+    hid = sizes[edge]
     cols = dnw_ref.shape[1]
     group, strip = 2 * cols, cols // 2
     bf16, f32 = jnp.bfloat16, jnp.float32
 
-    pair, half_z = lax.div(z, 2), lax.rem(z, 2)
-    edge = lax.rem(pair + half_z + 1, 2)
+    half_z = lax.rem(z, 2)
     zp = z + 1 - 2 * half_z
     zm = far - 1 - z
     zd = far - 1 - zp
@@ -109,7 +143,9 @@
         [rr * 2 + ee for ee in ends]
         for rr, ends in ((r, side), (1 - r, side), (r, (1 - y, 1 - half_z)), (1 - r, (1 - y, 1 - half_z)))
     )
-    q_own, q_other = r * 2 + edge, r * 2 + 1 - edge
+
+    def split(kind):
+        return pl.ds(al(r * 16 * unit + kind * sizes[0], unit), sizes[kind])
 
     sibling = (r, z, y, 1 - t)
     beside = (r, z, 1 - y, t)
@@ -124,23 +160,31 @@
             src_ref=a, dst_ref=b, send_sem=s, recv_sem=q, device_id=where, device_id_type=pl.DeviceIdType.MESH
         )
 
-    def place(k, zs, ys):
+    def lines(k, size):
+        half = size // 2
+        return ((0, size), (0, half), (half, size - half))[k - 3]
+
+    def place(k, zs, ys, kind=None):
         p = zs * 2 + ys
         if k == 0:
             return trio.at[pl.ds(al(p * depth, depth), depth), :]
         if k == 1:
             return outb.at[:, pl.ds(al(p * cols, cols), cols)]
+        size = sizes[edge if kind is None else kind]
         if k == 2:
-            return upb.at[pl.ds(al(p * depth, depth), depth), :]
-        lo = ((zs * 2 + k - 3) * 2 + ys) * strip
-        return dnb.at[:, pl.ds(al(lo, strip), strip)]
+            return upb.at[pl.ds(al(p * depth, depth), depth), pl.ds(0, size)]
+        lo = ((zs * 2 + min(k - 3, 1)) * 2 + ys) * strip
+        top, some = lines(k, size)
+        return dnb.at[pl.ds(top, some), pl.ds(al(lo, strip), strip)]
 
     def share(k, q):
         if k == 1:
             return outw_ref.at[pl.ds(al(q * width, width), width), :]
         if k == 2:
-            return upw_ref.at[:, pl.ds(al(q * hid, hid), hid)]
-        return dnw_ref.at[pl.ds(al(q * hid, hid), hid), pl.ds((k - 3) * strip, strip)]
+            return upw_ref.at[:, split(q)]
+        top, some = lines(k, sizes[q])
+        start = al(r * 16 * unit + q * sizes[0] + top, unit)
+        return dnw_ref.at[pl.ds(start, some), pl.ds(min(k - 3, 1) * strip, strip)]
 
     def trio_copies(dst, q, sems):
         return [
@@ -155,8 +199,8 @@
     own_trio = trio_copies(place(0, z, y), r * 2 + y, local_sem)
     other_trio = trio_copies(stage, r * 2 + 1 - y, stage_sem)
     own_rest = [None] + [
-        pltpu.make_async_copy(share(k, r * 2 + y if k == 1 else q_own), place(k, z, y), local_sem.at[2 + k])
-        for k in (1, 2, 3, 4)
+        pltpu.make_async_copy(share(k, r * 2 + y if k == 1 else edge), place(k, z, y), local_sem.at[2 + k])
+        for k in (1, 2, 3, 4, 5)
     ]
 
     def near_copy(k):
@@ -191,19 +235,14 @@
         send_on(k, zs, ys)
 
     def w_copy(k, i):
-        a = share(k, q_own if i == 1 else q_other)
+        kind = edge if i == 1 else 1 - edge
         return push(
-            a, place(k, z, y), w_send.at[k - 2, i], w_recv.at[k, z * 2 + y], (r, (zp, zm, zd)[i], y, t)
+            share(k, kind), place(k, z, y, kind), w_send.at[k - 2, i], w_recv.at[k, z * 2 + y], (r, (zp, zm, zd)[i], y, t)
         )
-
-    def w_when(k, i, at_edge):
-        @pl.when(edge == at_edge)
-        def _():
-            w_copy(k, i).start()
 
     def y_copy(k, j):
         at = place(k, line[j], y)
-        a = share(k, q_own) if j == 0 else at
+        a = share(k, edge) if j == 0 else at
         return push(a, at, y_send.at[k - 2, j], w_recv.at[k, line[j] * 2 + y], beside)
 
     def landed(k, j, ys):
@@ -213,6 +252,15 @@
     def arrive(k, j):
         landed(k, j, y)
         y_copy(k, j).start()
+
+    def at(point):
+        for what, k, i in PLAN[edge].get(point, ()):
+            if what == SEND:
+                w_copy(k, i).start()
+            elif what == OWN:
+                y_copy(k, 0).start()
+            else:
+                arrive(k, i)
 
     def norm(values, gain_ref):
         inverse = lax.rsqrt(jnp.mean(values * values, axis=-1, keepdims=True) + eps)
@@ -310,34 +358,28 @@
     own_rest[1].wait()
     send_on(1, z, y)
     ag_start(0, toks)
+    at(0)
     for k in (0, 1):
         mix_landed(k, z, 1 - y)
-    w_when(2, 0, 1)
+    at(1)
     for k in (0, 1):
         for ys in (y, 1 - y):
             mix_landed(k, nth(1), ys)
+    at(2)
     for k in (0, 1):
         for ys in (y, 1 - y):
             mix_landed(k, nth(2), ys)
+    at(3)
     ag_relay(0, toks, pal[0], (3, 4))
     ag_relay(0, toks, cross[0], (5,))
-    y_copy(2, 0).start()
     for k in (0, 1):
         for ys in (y, 1 - y):
             mix_landed(k, nth(3), ys)
-    for k in (3, 4):
-        y_copy(k, 0).start()
-    w_when(2, 1, 0)
-    w_when(2, 2, 1)
+    at(4)
     ag_relay(0, toks, diag[0], (6,))
     for s in (own[0], cross[0], pal[0], diag[0]):
         ag_wait(0, toks, s, 1 - t)
-
-    w_when(2, 0, 0)
-
-    @pl.when(edge == 0)
-    def _():
-        arrive(2, 1)
+    at(5)
 
     mix_cols = outb.shape[1]
     taps = taps_ref[:, pl.ds(al((r * 2 + y) * width, width), width)]
@@ -364,57 +406,42 @@
         sib_copy(0, s, part, sib, 0, mix_cols).wait_recv()
     for n in range(far):
         reduce_x(0, n, n * group, group)
+    at(6)
     for s in (pal[0], own[0]):
         sib_copy(0, s, part, sib, 0, mix_cols).wait_recv()
     for n in range(far):
         reduce_p(0, n, n * group, group)
-        if n == 0:
-            w_when(2, 1, 1)
-            w_when(2, 2, 0)
-        if n == 2:
-            for k in (3, 4):
-                w_when(k, 0, 1)
-                w_when(k, 2, 1)
-
-    @pl.when(edge == 1)
-    def _():
-        arrive(2, 1)
-
+        at(7 + n)
     for n in range(far):
-        at = pl.ds(n * group, group)
+        span = pl.ds(n * group, group)
         total = reduce_end(0, n, n * group, group)
-        resid[:, at] = (tok_ref[:, at].astype(f32) + total).astype(bf16)
+        resid[:, span] = (tok_ref[:, span].astype(f32) + total).astype(bf16)
+    at(11)
     slot(toks_ff, own[1], t)[...] = norm(resid[...].astype(f32), ff_gain_ref)
     ag_start(1, toks_ff)
-    for j in (2, 3):
-        arrive(2, j)
-    for k in (3, 4):
-        w_when(k, 1, 0)
-        w_when(k, 0, 0)
+    at(12)
     ag_relay(1, toks_ff, pal[1], (3, 4))
+    at(13)
     ag_relay(1, toks_ff, cross[1], (5,))
-    arrive(3, 1)
-    w_when(3, 1, 1)
-    w_when(3, 2, 0)
+    at(14)
     own_rest[2].wait()
     for j in range(4):
         landed(2, j, 1 - y)
+    at(16)
 
     def up(i):
         s = seq_at(1, 3 - i)
         ag_wait(1, toks_ff, s, 1 - t)
         x = toks_ff[pl.ds(al(s * seq, seq), seq), :]
-        half = hid // 2
-        for lo in (0, half):
-            act = jnp.dot(x, upb[:, pl.ds(lo, half)], preferred_element_type=f32)
-            hidden[pl.ds(al(s * seq, seq), seq), pl.ds(lo, half)] = jnp.square(jnp.maximum(act, 0.0)).astype(bf16)
+        for lo, size in ((0, 4 * unit), (4 * unit, hid - 4 * unit)):
+            act = jnp.dot(x, upb[:, pl.ds(lo, size)], preferred_element_type=f32)
+            hidden[pl.ds(al(s * seq, seq), seq), pl.ds(lo, size)] = jnp.square(jnp.maximum(act, 0.0)).astype(bf16)
 
     pl.loop(0, 3)(up)
     ag_relay(1, toks_ff, diag[1], (6,))
-    arrive(4, 1)
-    w_when(4, 1, 1)
-    w_when(4, 2, 0)
+    at(17)
     up(3)
+    at(18)
 
     def down(j, h):
         m = line[j] * 2 + h
@@ -424,84 +451,127 @@
         def _(i):
             s = seq_at(1, i)
             part_ff[pl.ds(al(s * seq, seq), seq), pl.ds(lo, cols)] = jnp.dot(
-                hidden[pl.ds(al(s * seq, seq), seq), :], dnb[:, pl.ds(lo, cols)], preferred_element_type=f32
+                hidden[pl.ds(al(s * seq, seq), seq), pl.ds(0, hid)],
+                dnb[pl.ds(0, hid), pl.ds(lo, cols)],
+                preferred_element_type=f32,
             ).astype(bf16)
             sib_copy(1 + m, s, part_ff, sib_ff, lo, cols).start()
 
+    def spread(j, h):
+        m = line[j] * 2 + h
+        lo = al(m * cols, cols)
         for s in (diag[1], cross[1]):
             sib_copy(1 + m, s, part_ff, sib_ff, lo, cols).wait_recv()
         reduce_x(1, far + m, lo, cols)
+
+    def finish(j, h):
+        m = line[j] * 2 + h
+        lo = al(m * cols, cols)
         for s in (pal[1], own[1]):
             sib_copy(1 + m, s, part_ff, sib_ff, lo, cols).wait_recv()
-
-    def finish(j, h):
-        m = line[j] * 2 + h
-        reduce_p(1, far + m, al(m * cols, cols), cols)
+        reduce_p(1, far + m, lo, cols)
+
+    def out_copy(j, h, ys):
+        span = pl.ds(al(line[j] * group + ys * cols + h * strip, strip), strip)
+        return pltpu.make_async_copy(result.at[:, span], o_ref.at[:, span], out_sem.at[(j * 2 + h) * 2 + ys])
 
     def end(j, h):
         m = line[j] * 2 + h
         total = reduce_end(1, far + m, al(m * cols, cols), cols)
         for ys in range(2):
-            at = pl.ds(al(line[j] * group + ys * cols + h * strip, strip), strip)
-            o_ref[:, at] = (resid[:, at].astype(f32) + total[:, ys * strip : (ys + 1) * strip]).astype(bf16)
+            span = pl.ds(al(line[j] * group + ys * cols + h * strip, strip), strip)
+            result[:, span] = (resid[:, span].astype(f32) + total[:, ys * strip : (ys + 1) * strip]).astype(bf16)
+            out_copy(j, h, ys).start()
 
     own_rest[3].wait()
     own_rest[4].wait()
-    steps = [(0, 0), (0, 1), (1, 0), (1, 1), (2, 0), (3, 0), (2, 1), (3, 1)]
-    ahead = {0: ((3, 2), (3, 3)), 2: ((4, 2),), 3: ((4, 3),)}
-    for n, (j, h) in enumerate(steps):
-        landed(3 + h, j, 1 - y)
-        down(j, h)
-        for block in ahead.get(n, ()):
-            arrive(*block)
-        if n > 0:
-            finish(*steps[n - 1])
-        if n > 2:
-            end(*steps[n - 3])
-    finish(*steps[-1])
-    for step in steps[-3:]:
-        end(*step)
-
-    for k in (0, 1):
-        near_copy(k).wait_send()
-        for zs in range(far):
-            for ys in range(2):
-                @pl.when(jnp.logical_and(zs <= z, z + 1 < far))
-                def _():
-                    hop(k, zs, ys, 1, right_send).wait_send()
-
-                @pl.when(jnp.logical_and(zs >= z, z > 0))
-                def _():
-                    hop(k, zs, ys, -1, left_send).wait_send()
-    for k in (2, 3, 4):
-        for i in range(3):
-            w_copy(k, i).wait_send()
-        for j in range(4):
-            y_copy(k, j).wait_send()
-    for g, buf in ((0, toks), (1, toks_ff)):
-        for i in range(7):
-            ag_copy(g, buf, i).wait_send()
-    for s in range(4):
-        sib_copy(0, s, part, sib, 0, mix_cols).wait_send()
-    for n in range(far):
-        lo = n * group
-        for j in range(2):
-            x_copy(n, j, xs, xr, lo, group).wait_send()
-        p_copy(0, n, ps, pr, lo, group).wait_send()
-    for m in range(2 * far):
-        lo = m * cols
+    own_rest[5].wait()
+    def sent_mixer():
+        for k in (0, 1):
+            near_copy(k).wait_send()
+            for zs in range(far):
+                for ys in range(2):
+                    @pl.when(jnp.logical_and(zs <= z, z + 1 < far))
+                    def _():
+                        hop(k, zs, ys, 1, right_send).wait_send()
+
+                    @pl.when(jnp.logical_and(zs >= z, z > 0))
+                    def _():
+                        hop(k, zs, ys, -1, left_send).wait_send()
+        for g, buf in ((0, toks), (1, toks_ff)):
+            for i in range(7):
+                ag_copy(g, buf, i).wait_send()
+        for s in range(4):
+            sib_copy(0, s, part, sib, 0, mix_cols).wait_send()
+        for n in range(far):
+            lo = n * group
+            for j in range(2):
+                x_copy(n, j, xs, xr, lo, group).wait_send()
+            p_copy(0, n, ps, pr, lo, group).wait_send()
+
+    def sent_weights(ks):
+        for k in ks:
+            for i in range(3):
+                w_copy(k, i).wait_send()
+            for j in range(4):
+                y_copy(k, j).wait_send()
+
+    def sent_step(j, h):
+        m = line[j] * 2 + h
+        lo = al(m * cols, cols)
         for s in range(4):
             sib_copy(1 + m, s, part_ff, sib_ff, lo, cols).wait_send()
-        for j in range(2):
-            x_copy(far + m, j, xs_ff, xr_ff, lo, cols).wait_send()
+        for i in range(2):
+            x_copy(far + m, i, xs_ff, xr_ff, lo, cols).wait_send()
         p_copy(1, far + m, ps_ff, pr_ff, lo, cols).wait_send()
+
+    steps = [(0, 0), (0, 1), (1, 0), (1, 1), (2, 0), (3, 0), (2, 1), (3, 1)]
+    late = LATE
+    for n, (j, h) in enumerate(steps):
+        if n >= late:
+            spread(*steps[n - 1])
+        if n == 6:
+            sent_mixer()
+        if n == 7:
+            sent_weights((2,))
+            for step in steps[:4]:
+                sent_step(*step)
+        for k in ((3,), (4, 5))[h]:
+            landed(k, j, 1 - y)
+        down(j, h)
+        at(19 + n)
+        if 0 < n < late:
+            spread(*steps[n - 1])
+        if n > 1:
+            finish(*steps[n - 2])
+        if n > 4:
+            end(*steps[n - 5])
+    spread(*steps[-1])
+    finish(*steps[-2])
+    finish(*steps[-1])
+    for step in steps[-5:]:
+        end(*step)
+
+    for j, h in steps:
+        for ys in range(2):
+            out_copy(j, h, ys).wait()
+    sent_weights((3, 4, 5))
+    for step in steps[4:]:
+        sent_step(*step)
+
+
+def layer_kernel(far, *refs):
+    z = lax.axis_index("far")
+    inside = lax.rem(lax.div(z, 2) + lax.rem(z, 2), 2) == 1
+    pl.when(inside)(functools.partial(chip_kernel, far, 0, *refs))
+    pl.when(jnp.logical_not(inside))(functools.partial(chip_kernel, far, 1, *refs))
 
 
 def fused_layer(far, tokens, mix_gain, conv_in, outer, inner, taps, out_w, ff_gain, up_w, down_w):
     bf16 = jnp.bfloat16
     rows, feat = tokens.shape
     depth, cols = up_w.shape[0], down_w.shape[1]
-    width, hid = conv_in.shape[1] // 4, up_w.shape[1] // 4
+    width, hid = conv_in.shape[1] // 4, up_w.shape[1] * 8 // 32
     whole = 8 * rows
     vmem = pl.BlockSpec(memory_space=pltpu.VMEM)
     hbm = pl.BlockSpec(memory_space=pl.ANY)
@@ -518,7 +588,7 @@
         functools.partial(layer_kernel, far),
         out_shape=jax.ShapeDtypeStruct((rows, feat), bf16),
         in_specs=[vmem, vmem, hbm, hbm, hbm, vmem, hbm, vmem, hbm, hbm],
-        out_specs=vmem,
+        out_specs=hbm,
         scratch_shapes=[
             pltpu.VMEM((far * 2 * depth, 3 * width), bf16),
             pltpu.VMEM((width, far * 2 * cols), bf16),
@@ -531,14 +601,16 @@
             *block,
             pltpu.VMEM((whole, hid), bf16),
             pltpu.VMEM((rows, feat), bf16),
-            dma((7,)),
+            pltpu.VMEM((rows, feat), bf16),
+            dma((16,)),
+            dma((8,)),
             dma((3,)),
             dma((2,)),
             dma((2, far * 2)),
             dma((2, far * 2)),
-            dma((3, 3)),
-            dma((3, 4)),
-            dma((5, far * 2)),
+            dma((4, 3)),
+            dma((4, 4)),
+            dma((6, far * 2)),
             dma((2, 7)),
             dma((2, 8)),
             dma((1 + 2 * far, 4)),

time: 160 us -> 155 us (0.969)
  Pallas kernels: 158 us -> 153 us
    pallas_call x1, Pallas kernels: 158 us -> 153 us  [fused_layer(): pl.pallas_call(functools.partial(layer_kernel, far), out_shape=jax.ShapeD...]
where the time goes in v3:
time: 155 us
  Pallas kernels  153 us (99%)
  local copies, waits for them, and re-layouts  1.88 us (1%)
    pallas_call x1, Pallas kernels, fused_layer(): pl.pallas_call(functools.partial(layer_kernel, far), out_shape=jax.ShapeD...  153 us

profile of v3, /device:TPU:0, one launch (start us, length us, event | category | flops | bytes accessed | tf_op | source)
XLA Modules:
  0.0 154.7 jit_solution(7336578706428160154)
XLA Ops:
  0.0 152.8 %shard_map.100 = bf16[128,2048]{1,0:T(8,128)(2,1)} custom-call(bf16[128,2048]{1,0:T(8,128)(2,1)} %refs_0_.1, f32[1,2048]{1,0:T(1,128)} %bitcast.2, bf16[256,512]{1,0:T(8,128)(2,1)} %refs_2_.1, bf16[256,512]{1,0:T(8,128)(2,1)} %refs_3_.1, bf16[256,512]{1,0:T(8,128)(2,1)} %refs_4_.1, f32[3,512]{1,0:T(4,128)} %refs_5_.1, bf16[512,256]{1,0:T(8,128)(2,1)} %refs_6_.1, ...), custom_call_target="tpu_custom_call" | custom-call | tf_op jit(solution)/shard_map/pallas_call | solution.py:587
  152.8 1.9 %copy.12 = bf16[128,2048]{1,0:T(8,128)(2,1)} copy(bf16[128,2048]{1,0:T(8,128)(2,1)} %shard_map.100) | data formatting | bytes 1048576

commit v4 on v3

--- a/solution.py
+++ b/solution.py
@@ -75,7 +75,7 @@
     return (resid.astype(jnp.float32) + project(hidden, down_full)).astype(jnp.bfloat16)
 
 
-SEND, OWN, TAKE = range(3)
+SEND, OWN, TAKE, LEND, PASS = range(5)
 LATE = 6
 PLAN = (
     {
@@ -83,27 +83,35 @@
         4: ((SEND, 2, 1), (SEND, 2, 0),),
         5: ((TAKE, 2, 1),),
         7: ((SEND, 2, 2),),
-        12: ((TAKE, 2, 2), (TAKE, 2, 3), (SEND, 3, 0), (SEND, 3, 1),),
-        13: ((SEND, 3, 2),),
-        14: ((TAKE, 3, 1), (SEND, 4, 0), (SEND, 5, 0), (SEND, 4, 1), (SEND, 5, 1), (SEND, 4, 2), (SEND, 5, 2),),
-        19: ((TAKE, 4, 1), (TAKE, 5, 1),),
-        20: ((TAKE, 3, 2), (TAKE, 3, 3),),
-        22: ((TAKE, 4, 2), (TAKE, 5, 2),),
-        23: ((TAKE, 4, 3), (TAKE, 5, 3),),
+        10: ((TAKE, 2, 2), (TAKE, 2, 3),),
+        12: ((SEND, 3, 0), (SEND, 3, 1), (SEND, 3, 2), (SEND, 4, 1), (SEND, 5, 1), (SEND, 4, 2), (SEND, 5, 2), (SEND, 4, 0), (SEND, 5, 0), (TAKE, 3, 1), (TAKE, 4, 1), (TAKE, 5, 1),),
+        14: ((TAKE, 3, 2),),
+        16: ((TAKE, 3, 3),),
+        21: ((TAKE, 4, 2),),
+        22: ((TAKE, 5, 2), (TAKE, 4, 3),),
+        23: ((TAKE, 5, 3),),
     },
     {
-        1: ((SEND, 2, 0),),
-        2: ((SEND, 2, 2), (OWN, 2, 0), (OWN, 3, 0), (OWN, 4, 0), (OWN, 5, 0),),
-        3: ((SEND, 3, 0), (SEND, 4, 0), (SEND, 5, 0),),
+        1: ((LEND, 0, 0), (SEND, 2, 0),),
+        2: ((OWN, 2, 0), (OWN, 3, 0), (OWN, 4, 0), (OWN, 5, 0),),
+        3: ((SEND, 2, 2), (PASS, 0, 0), (SEND, 3, 0), (SEND, 4, 0), (SEND, 5, 0),),
         6: ((TAKE, 2, 1), (SEND, 2, 1),),
-        12: ((TAKE, 2, 2), (TAKE, 2, 3), (SEND, 3, 2),),
-        13: ((SEND, 3, 1),),
-        14: ((TAKE, 3, 1), (SEND, 4, 1), (SEND, 5, 1), (SEND, 4, 2), (SEND, 5, 2),),
-        19: ((TAKE, 4, 1), (TAKE, 5, 1),),
-        20: ((TAKE, 3, 2), (TAKE, 3, 3),),
-        22: ((TAKE, 4, 2), (TAKE, 5, 2),),
-        23: ((TAKE, 4, 3), (TAKE, 5, 3),),
+        12: ((TAKE, 2, 2), (TAKE, 2, 3), (SEND, 3, 2), (SEND, 3, 1),),
+        13: ((SEND, 4, 2), (SEND, 5, 2), (SEND, 4, 1), (SEND, 5, 1),),
+        14: ((TAKE, 3, 1),),
+        16: ((TAKE, 3, 2),),
+        17: ((TAKE, 3, 3),),
+        18: ((TAKE, 4, 1),),
+        19: ((TAKE, 5, 1),),
+        20: ((TAKE, 4, 2),),
+        21: ((TAKE, 5, 2),),
+        22: ((TAKE, 4, 3),),
+        23: ((TAKE, 5, 3),),
     },
+)
+STEPS = (
+    ((0, 0), (0, 1), (1, 0), (1, 1), (2, 0), (3, 0), (2, 1), (3, 1)),
+    ((0, 0), (0, 1), (1, 0), (2, 0), (3, 0), (1, 1), (2, 1), (3, 1)),
 )
 
 
@@ -117,7 +125,7 @@
     o_ref,
     trio, outb, upb, dnb, stage, toks, toks_ff,
     part, sib, xs, xr, ps, pr, part_ff, sib_ff, xs_ff, xr_ff, ps_ff, pr_ff,
-    hidden, resid, result, out_sem,
+    hidden, resid, result, out_sem, swap, swap_sem,
     local_sem, stage_sem, near_send, right_send, left_send, w_send, y_send, w_recv,
     ag_send, ag_recv, sib_send, sib_recv, x_send, x_recv, p_send, p_recv,
 ):
@@ -127,7 +135,7 @@
     width = trio.shape[1] // 3
     depth = upw_ref.shape[0]
     unit = upw_ref.shape[1] // 32
-    sizes = (8 * unit, 8 * unit)
+    sizes = (9 * unit, 7 * unit)
     hid = sizes[edge]
     cols = dnw_ref.shape[1]
     group, strip = 2 * cols, cols // 2
@@ -161,7 +169,7 @@
         )
 
     def lines(k, size):
-        half = size // 2
+        half = size // (2 * unit) * unit
         return ((0, size), (0, half), (half, size - half))[k - 3]
 
     def place(k, zs, ys, kind=None):
@@ -249,9 +257,19 @@
         at = place(k, line[j], ys)
         push(at, at, y_send.at[k - 2, j], w_recv.at[k, line[j] * 2 + ys], beside).wait_recv()
 
+    def through(k, j):
+        return edge == 0 and k == 2 and j == 1
+
     def arrive(k, j):
         landed(k, j, y)
-        y_copy(k, j).start()
+        if not through(k, j):
+            y_copy(k, j).start()
+
+    def lend():
+        return push(share(2, 0), swap, swap_sem.at[0], swap_sem.at[1], beside)
+
+    def lent():
+        return push(swap, place(2, z, 1 - y, 0), swap_sem.at[2], w_recv.at[2, z * 2 + 1 - y], partner[1])
 
     def at(point):
         for what, k, i in PLAN[edge].get(point, ()):
@@ -259,8 +277,13 @@
                 w_copy(k, i).start()
             elif what == OWN:
                 y_copy(k, 0).start()
+            elif what == TAKE:
+                arrive(k, i)
+            elif what == LEND:
+                lend().start()
             else:
-                arrive(k, i)
+                lend().wait_recv()
+                lent().start()
 
     def norm(values, gain_ref):
         inverse = lax.rsqrt(jnp.mean(values * values, axis=-1, keepdims=True) + eps)
@@ -514,7 +537,8 @@
             for i in range(3):
                 w_copy(k, i).wait_send()
             for j in range(4):
-                y_copy(k, j).wait_send()
+                if not through(k, j):
+                    y_copy(k, j).wait_send()
 
     def sent_step(j, h):
         m = line[j] * 2 + h
@@ -525,7 +549,7 @@
             x_copy(far + m, i, xs_ff, xr_ff, lo, cols).wait_send()
         p_copy(1, far + m, ps_ff, pr_ff, lo, cols).wait_send()
 
-    steps = [(0, 0), (0, 1), (1, 0), (1, 1), (2, 0), (3, 0), (2, 1), (3, 1)]
+    steps = STEPS[edge]
     late = LATE
     for n, (j, h) in enumerate(steps):
         if n >= late:
@@ -544,18 +568,19 @@
             spread(*steps[n - 1])
         if n > 1:
             finish(*steps[n - 2])
-        if n > 4:
-            end(*steps[n - 5])
     spread(*steps[-1])
     finish(*steps[-2])
     finish(*steps[-1])
-    for step in steps[-5:]:
+    for step in steps:
         end(*step)
 
     for j, h in steps:
         for ys in range(2):
             out_copy(j, h, ys).wait()
     sent_weights((3, 4, 5))
+    if edge == 1:
+        lend().wait_send()
+        lent().wait_send()
     for step in steps[4:]:
         sent_step(*step)
 
@@ -571,7 +596,7 @@
     bf16 = jnp.bfloat16
     rows, feat = tokens.shape
     depth, cols = up_w.shape[0], down_w.shape[1]
-    width, hid = conv_in.shape[1] // 4, up_w.shape[1] * 8 // 32
+    width, hid = conv_in.shape[1] // 4, up_w.shape[1] * 9 // 32
     whole = 8 * rows
     vmem = pl.BlockSpec(memory_space=pltpu.VMEM)
     hbm = pl.BlockSpec(memory_space=pl.ANY)
@@ -603,6 +628,8 @@
             pltpu.VMEM((rows, feat), bf16),
             pltpu.VMEM((rows, feat), bf16),
             dma((16,)),
+            pltpu.VMEM((depth, hid), bf16),
+            dma((3,)),
             dma((8,)),
             dma((3,)),
             dma((2,)),

time: 155 us -> 148 us (0.955)
  Pallas kernels: 153 us -> 146 us
    pallas_call x1, Pallas kernels: 153 us -> 146 us  [fused_layer(): pl.pallas_call(functools.partial(layer_kernel, far), out_shape=jax.ShapeD...]
where the time goes in v4:
time: 148 us; the launch traced here: 147 us
  Pallas kernels  146 us (99%)
  local copies, waits for them, and re-layouts  1.88 us (1%)
    pallas_call x1, Pallas kernels, fused_layer(): pl.pallas_call(functools.partial(layer_kernel, far), out_shape=jax.ShapeD...  146 us

profile of v4, /device:TPU:0, one launch (start us, length us, event | category | flops | bytes accessed | tf_op | source)
XLA Modules:
  0.0 147.5 jit_solution(15758881840080423991)
XLA Ops:
  0.0 145.6 %shard_map.100 = bf16[128,2048]{1,0:T(8,128)(2,1)} custom-call(bf16[128,2048]{1,0:T(8,128)(2,1)} %refs_0_.1, f32[1,2048]{1,0:T(1,128)} %bitcast.2, bf16[256,512]{1,0:T(8,128)(2,1)} %refs_2_.1, bf16[256,512]{1,0:T(8,128)(2,1)} %refs_3_.1, bf16[256,512]{1,0:T(8,128)(2,1)} %refs_4_.1, f32[3,512]{1,0:T(4,128)} %refs_5_.1, bf16[512,256]{1,0:T(8,128)(2,1)} %refs_6_.1, ...), custom_call_target="tpu_custom_call" | custom-call | tf_op jit(solution)/shard_map/pallas_call | solution.py:612
  145.6 1.9 %copy.12 = bf16[128,2048]{1,0:T(8,128)(2,1)} copy(bf16[128,2048]{1,0:T(8,128)(2,1)} %shard_map.100) | data formatting | bytes 1048576

commit v5 on v4

--- a/solution.py
+++ b/solution.py
@@ -96,7 +96,8 @@
         2: ((OWN, 2, 0), (OWN, 3, 0), (OWN, 4, 0), (OWN, 5, 0),),
         3: ((SEND, 2, 2), (PASS, 0, 0), (SEND, 3, 0), (SEND, 4, 0), (SEND, 5, 0),),
         6: ((TAKE, 2, 1), (SEND, 2, 1),),
-        12: ((TAKE, 2, 2), (TAKE, 2, 3), (SEND, 3, 2), (SEND, 3, 1),),
+        11: ((TAKE, 2, 2),),
+        12: ((TAKE, 2, 3), (SEND, 3, 2), (SEND, 3, 1),),
         13: ((SEND, 4, 2), (SEND, 5, 2), (SEND, 4, 1), (SEND, 5, 1),),
         14: ((TAKE, 3, 1),),
         16: ((TAKE, 3, 2),),

time: 148 us -> 148 us (level)
  no operation moved by 1% of the time
where the time goes in v5:
time: 148 us; the launch traced here: 147 us
  Pallas kernels  146 us (99%)
  local copies, waits for them, and re-layouts  1.88 us (1%)
    pallas_call x1, Pallas kernels, fused_layer(): pl.pallas_call(functools.partial(layer_kernel, far), out_shape=jax.ShapeD...  146 us

profile of v5, /device:TPU:0, one launch (start us, length us, event | category | flops | bytes accessed | tf_op | source)
XLA Modules:
  0.0 147.4 jit_solution(14594523669665905344)
XLA Ops:
  0.0 145.6 %shard_map.100 = bf16[128,2048]{1,0:T(8,128)(2,1)} custom-call(bf16[128,2048]{1,0:T(8,128)(2,1)} %refs_0_.1, f32[1,2048]{1,0:T(1,128)} %bitcast.2, bf16[256,512]{1,0:T(8,128)(2,1)} %refs_2_.1, bf16[256,512]{1,0:T(8,128)(2,1)} %refs_3_.1, bf16[256,512]{1,0:T(8,128)(2,1)} %refs_4_.1, f32[3,512]{1,0:T(4,128)} %refs_5_.1, bf16[512,256]{1,0:T(8,128)(2,1)} %refs_6_.1, ...), custom_call_target="tpu_custom_call" | custom-call | tf_op jit(solution)/shard_map/pallas_call | solution.py:613
  145.6 1.9 %copy.12 = bf16[128,2048]{1,0:T(8,128)(2,1)} copy(bf16[128,2048]{1,0:T(8,128)(2,1)} %shard_map.100) | data formatting | bytes 1048576
